TPU v7x, 32 devices: a whole 2x2x4 slice. The times are simulated.
32 devices in a mesh: sp: 16 (over z, y, x), tp: 2 (over core).
Axes of the slice: x: 2, y: 2, z: 4, core: 2. Of those that a mesh axis runs over, the one named last changes fastest.
Arguments:
- tokens: bfloat16 [8192, 2048], P('sp', 'tp'), may hold values from -6 to 6
- input_gain: bfloat16 [2048], P('tp'), may hold values from 0.099609375 to 1.8984375
- query_weight: bfloat16 [2048, 1024], P(None, 'tp'), may hold values from -10 to 10
- key_weight: bfloat16 [2048, 1024], P(None, 'tp'), may hold values from -10 to 10
- value_weight: bfloat16 [2048, 1024], P(None, 'tp'), may hold values from -0.125 to 0.125
- pool_in_weight: bfloat16 [2048, 1024], P(None, 'tp'), may hold values from -0.125 to 0.125
- log_gates: float32 [8, 8192], P('tp'), may hold values from -8192 to 0, as said below
- pool_weight: bfloat16 [8, 128, 128], P('tp'), may hold values from -0.5 to 0.5
- pool_scale: float32 [1024], P('tp'), may hold values from 0.1 to 1.9
- attention_out: bfloat16 [1024, 2048], P('tp'), may hold values from -16 to 16
- pooling_out: bfloat16 [1024, 2048], P('tp'), may hold values from -16 to 16
- final_gain: float32 [2048], P('tp'), may hold values from 0.1 to 1.9
Outputs:
- layer_out: bfloat16 [8192, 2048], P('sp', 'tp')
Inputs may be any that keep to these rules, and one draw needn't show every extreme that they name: `log_gates`: each row does not increase along positions.
All inputs are finite; a program needn't handle non-finite values.
Results may differ from a plain program's by a relative error of at most 0.015.
Values may be sent and summed in bfloat16 or wider, within the bound.
A program may use at most 128 MiB of HBM per device.

v0:
```python
import functools

import jax
import jax.numpy as jnp
from jax import lax
from jax.experimental import pallas as pl
from jax.experimental.pallas import tpu as pltpu
from jax.sharding import PartitionSpec as P


WINDOW_MAX = 16
LANES = 128
LOG2E = 1.4426950408889634

very_low = -1e30
epsilon = 1e-06


def passed_along(block, axis, distance):
    devices = range(lax.axis_size(axis))
    route = [(i - distance, i) for i in devices if i - distance in devices]
    return lax.ppermute(block, axis, route)


def swapped(block, axis, offset):
    return lax.ppermute(block, axis, [(i, i ^ offset) for i in range(lax.axis_size(axis))])


def attend_kernel(first, last, heads, head_size, chunk, mode_ref, start_ref, *refs):
    if first:
        q_ref, kv_ref, gate_ref, acc_out, ml_out = refs
    else:
        q_ref, kv_ref, gate_ref, acc_in, ml_in, acc_out, ml_out = refs
    slot = pl.program_id(0)
    rows = q_ref.shape[1]
    keys = kv_ref.shape[0]
    width = heads * head_size
    lane = lax.broadcasted_iota(jnp.int32, (chunk, LANES), 1)

    def state_of(r, h):
        if first:
            return None
        ml = ml_in[0, r : r + chunk, :]
        columns = slice(h * head_size, (h + 1) * head_size)
        return (ml[:, h : h + 1], ml[:, heads + h : heads + h + 1], acc_in[0, r : r + chunk, columns])

    def store(r, h, ml, state):
        columns = slice(h * head_size, (h + 1) * head_size)
        high, total, summed = state
        if last:
            safe = jnp.where(total > 0.0, total, 1.0)
            acc_out[0, r : r + chunk, columns] = (summed / safe).astype(acc_out.dtype)
            level = jnp.where(total > 0.0, high + jnp.log2(safe), very_low)
            return jnp.where(lane == h, level, ml)
        acc_out[0, r : r + chunk, columns] = summed
        return jnp.where(lane == h, high, jnp.where(lane == heads + h, total, ml))

    def compute(diagonal):
        for r in range(0, rows, chunk):
            ml = jnp.zeros((chunk, LANES), jnp.float32)
            span = min(r + chunk, keys) if diagonal else keys
            for h in range(heads):
                columns = slice(h * head_size, (h + 1) * head_size)
                q = q_ref[0, r : r + chunk, columns]
                k = kv_ref[:span, columns]
                v = kv_ref[:span, width + h * head_size : width + (h + 1) * head_size]
                bias = (start_ref[slot * heads + h] - gate_ref[h : h + 1, :span]) * LOG2E
                s = lax.dot_general(q, k, (((1,), (1,)), ((), ())), preferred_element_type=jnp.float32)
                s = s + bias
                if diagonal:
                    row = r + lax.broadcasted_iota(jnp.int32, s.shape, 0)
                    s = jnp.where(row >= lax.broadcasted_iota(jnp.int32, s.shape, 1), s, very_low)
                old = state_of(r, h)
                high = jnp.max(s, axis=1, keepdims=True)
                if old is not None:
                    high = jnp.maximum(high, old[0])
                p = jnp.exp2(s - high)
                total = jnp.sum(p, axis=1, keepdims=True)
                summed = jnp.dot(p.astype(jnp.bfloat16), v, preferred_element_type=jnp.float32)
                if old is not None:
                    factor = jnp.exp2(old[0] - high)
                    total = total + factor * old[1]
                    summed = summed + factor * old[2]
                ml = store(r, h, ml, (high, total, summed))
            ml_out[0, r : r + chunk, :] = ml

    if first:
        pl.when(slot == 0)(lambda: compute(True))

        @pl.when((slot > 0) & (mode_ref[slot] > 0))
        def _():
            compute(False)

    else:

        @pl.when(mode_ref[slot] > 0)
        def _():
            compute(False)

    @pl.when((mode_ref[slot] == 0) & ((slot > 0) | (not first)))
    def _():
        for r in range(0, rows, chunk):
            ml = jnp.zeros((chunk, LANES), jnp.float32)
            for h in range(heads):
                old = state_of(r, h)
                if old is None:
                    old = (
                        jnp.full((chunk, 1), very_low, jnp.float32),
                        jnp.zeros((chunk, 1), jnp.float32),
                        jnp.zeros((chunk, head_size), jnp.float32),
                    )
                ml = store(r, h, ml, old)
            ml_out[0, r : r + chunk, :] = ml


def attend_step(mode, starts, queries, pair, gates, state, last, head_size):
    slots, rows, width = queries.shape
    heads = width // head_size
    first = state is None
    chunk = min(rows, 256)
    by_slot = lambda g, *_: (g, 0, 0)
    whole = lambda g, *_: (0, 0)
    in_specs = [
        pl.BlockSpec((1, rows, width), by_slot),
        pl.BlockSpec(pair.shape, whole),
        pl.BlockSpec(gates.shape, whole),
    ]
    state_specs = [pl.BlockSpec((1, rows, width), by_slot), pl.BlockSpec((1, rows, LANES), by_slot)]
    if not first:
        in_specs = in_specs + state_specs
    keys = pair.shape[0]
    return pl.pallas_call(
        functools.partial(attend_kernel, first, last, heads, head_size, chunk),
        out_shape=(
            jax.ShapeDtypeStruct((slots, rows, width), jnp.bfloat16 if last else jnp.float32),
            jax.ShapeDtypeStruct((slots, rows, LANES), jnp.float32),
        ),
        grid_spec=pltpu.PrefetchScalarGridSpec(
            num_scalar_prefetch=2, grid=(slots,), in_specs=in_specs, out_specs=state_specs
        ),
        compiler_params=pltpu.CompilerParams(dimension_semantics=("arbitrary",)),
        cost_estimate=pl.CostEstimate(
            flops=8 * slots * rows * keys * width,
            bytes_accessed=12 * slots * rows * width,
            transcendentals=slots * rows * keys * heads,
        ),
    )(mode, starts, queries, pair, gates, *(() if first else state))


MESH = pl.DeviceIdType.MESH
SUB_ROWS = 128


def exchange_kernel(
    planes, seats, q_ref, k_ref, v_ref, gate_ref, out_ref,
    keys, values, queries, results, acc, high,
    z_send, z_recv, x_send, x_recv, y_send, y_recv, r_send, r_recv, o_send, o_recv,
):
    rows, head_size = queries.shape[1:]
    me = lax.axis_index("sp")
    plane, seat = me // seats, me % seats
    across = seat + 1 - 2 * (seat % 2)
    along = seat + 2 - 4 * (seat // 2)
    far = 3 - seat

    def device(p, s):
        return {"sp": p * seats + s}

    def block_rows(p, s):
        return pl.ds(pl.multiple_of((p * seats + s) * rows, rows), rows)

    def columns(p):
        return pl.ds(pl.multiple_of(p * head_size, head_size), head_size)

    def key_at(p, s):
        return keys.at[block_rows(p, s), :]

    def value_at(p, s):
        return values.at[block_rows(p, s), pl.ds(0, head_size)]

    def copy(source, target, send, recv, p, s):
        return pltpu.make_async_remote_copy(
            src_ref=source, dst_ref=target, send_sem=send, recv_sem=recv,
            device_id=device(p, s), device_id_type=MESH,
        )

    barrier = pltpu.get_barrier_semaphore()
    for d in range(1, planes):
        pl.semaphore_signal(barrier, inc=1, device_id=device((plane + d) % planes, seat), device_id_type=MESH)
    for s in (across, along):
        pl.semaphore_signal(barrier, inc=1, device_id=device(plane, s), device_id_type=MESH)
    pl.semaphore_wait(barrier, planes + 1)

    def from_plane(d):
        return (plane + planes - d) % planes

    def query_copy(d):
        to = (plane + d) % planes
        return copy(q_ref.at[:, columns(to)], queries.at[plane], z_send.at[0, d], z_recv.at[0, d], to, seat)

    def pair_copies(d):
        to = (plane + d) % planes
        return (
            copy(k_ref.at[:, columns(to)], key_at(plane, seat), z_send.at[1, d], z_recv.at[1, d], to, seat),
            copy(v_ref.at[:, columns(to)], value_at(plane, seat), z_send.at[2, d], z_recv.at[2, d], to, seat),
        )

    def spread(d, own):
        p = from_plane(d)
        k = k_ref.at[:, columns(plane)] if own else key_at(p, seat)
        v = v_ref.at[:, columns(plane)] if own else value_at(p, seat)
        return (
            copy(k, key_at(p, seat), x_send.at[0, d], x_recv.at[0, d], plane, across),
            copy(v, value_at(p, seat), y_send.at[1, d], y_recv.at[1, d], plane, along),
            copy(v, value_at(p, seat), x_send.at[1, d], x_recv.at[1, d], plane, across),
            copy(k, key_at(p, seat), y_send.at[0, d], y_recv.at[0, d], plane, along),
        )

    def relays(d):
        p = from_plane(d)
        return (
            copy(key_at(p, across), key_at(p, across), r_send.at[0, d], r_recv.at[0, d], plane, along),
            copy(value_at(p, along), value_at(p, along), r_send.at[1, d], r_recv.at[1, d], plane, across),
        )

    def arrival(target, recv):
        pltpu.make_async_remote_copy(
            src_ref=target, dst_ref=target, send_sem=z_send.at[0, 0], recv_sem=recv,
            device_id=device(plane, across), device_id_type=MESH,
        ).wait_recv()

    for d in range(1, planes):
        query_copy(d).start()
    for d in range(1, planes):
        for c in pair_copies(d):
            c.start()
    for c in spread(0, True):
        c.start()

    values[:, head_size:] = jnp.ones((values.shape[0], head_size), values.dtype)
    keys[block_rows(plane, seat), :] = k_ref[:, columns(plane)]
    values[block_rows(plane, seat), :head_size] = v_ref[:, columns(plane)]
    queries[plane] = q_ref[:, columns(plane)]
    acc[...] = jnp.zeros_like(acc)
    high[...] = jnp.full_like(high, very_low)

    def forward(d):
        p = from_plane(d)
        arrival(key_at(p, seat), z_recv.at[1, d])
        arrival(value_at(p, seat), z_recv.at[2, d])
        for c in spread(d, False):
            c.start()

    def relay(d):
        p = from_plane(d)
        to_along, to_across = relays(d)
        arrival(key_at(p, across), x_recv.at[0, d])
        to_along.start()
        arrival(value_at(p, along), y_recv.at[1, d])
        to_across.start()

    def settle(d):
        p = from_plane(d)
        arrival(value_at(p, across), x_recv.at[1, d])
        arrival(key_at(p, along), y_recv.at[0, d])
        arrival(key_at(p, far), r_recv.at[0, d])
        arrival(value_at(p, far), r_recv.at[1, d])

    span = seats * rows

    def head_gates(here):
        block = gate_ref[:, here]
        mine = lax.broadcasted_iota(jnp.int32, block.shape, 0) == plane
        return jnp.sum(jnp.where(mine, block, 0.0), axis=0, keepdims=True)

    def update(i, p, masked):
        here = pl.ds(pl.multiple_of(p * span, span), span)
        k = keys[here, :]
        v = values[here, :]
        gates = head_gates(here)
        start = head_gates(pl.ds(pl.multiple_of((i * seats + seat) * rows, rows), LANES))[:, :1]
        bias = (start - gates) * LOG2E
        scores = []
        for r in range(0, rows, SUB_ROWS):
            q = queries[i, r : r + SUB_ROWS, :]
            s = lax.dot_general(q, k, (((1,), (1,)), ((), ())), preferred_element_type=jnp.float32) + bias
            if masked:
                row = seat * rows + r + lax.broadcasted_iota(jnp.int32, s.shape, 0)
                s = jnp.where(row >= lax.broadcasted_iota(jnp.int32, s.shape, 1), s, very_low)
            scores.append(s)
        for n, r in enumerate(range(0, rows, SUB_ROWS)):
            s = scores[n]
            at = pl.ds(r, SUB_ROWS)
            old = high[i, at, :]
            new = jnp.maximum(old, jnp.max(s, axis=1, keepdims=True))
            p_ = jnp.exp2(s - new[:, :1]).astype(jnp.bfloat16)
            factor = jnp.exp2(old - new)
            summed = jnp.dot(p_, v, preferred_element_type=jnp.float32)
            acc[i, at, :] = acc[i, at, :] * jnp.concatenate([factor, factor], axis=1) + summed
            high[i, at, :] = new

    def finished(t):
        to = (plane + t) % planes
        return copy(results.at[to], out_ref.at[:, columns(plane)], o_send.at[t], o_recv.at[t], to, seat)

    relay(0)
    for d in range(1, planes):
        p = from_plane(d)
        arrival(queries.at[p], z_recv.at[0, d])

    def step(d, carry):
        @pl.when(d > 0)
        def _():
            relay(d)

        @pl.when(d < planes - 1)
        def _():
            forward(d + 1)

        settle(d)
        p = from_plane(d)

        def one(t, carry):
            i = (plane + t) % planes

            @pl.when(i > p)
            def _():
                update(i, p, False)

            @pl.when(i == p)
            def _():
                update(i, p, True)

            @pl.when(d == planes - 1)
            def _():
                result = (acc[i, :, :head_size] / acc[i, :, head_size:]).astype(jnp.bfloat16)

                @pl.when(t < planes)
                def _():
                    results[i] = result
                    finished(t).start()

                @pl.when(t == planes)
                def _():
                    out_ref[:, columns(plane)] = result

            return carry

        lax.fori_loop(1, planes + 1, one, 0)
        return carry

    lax.fori_loop(0, planes, step, 0)
    for t in range(1, planes):
        query_copy(t).wait_send()
        for c in pair_copies(t):
            c.wait_send()
    for c in spread(0, True):
        c.wait_send()
    for t in range(1, planes):
        for c in spread(t, False):
            c.wait_send()
    for t in range(planes):
        for c in relays(t):
            c.wait_send()
    for t in range(1, planes):
        finished(t).wait_send()
        arrival(out_ref.at[:, columns(from_plane(t))], o_recv.at[t])


def exchange_attend(query, keys, values, log_gates):
    rows, width = query.shape
    planes = log_gates.shape[0]
    seats = lax.axis_size("sp") // planes
    head_size = width // planes
    blocks = planes * seats
    dma = pltpu.SemaphoreType.DMA
    pairs = blocks * (blocks + 1) // 2
    return pl.pallas_call(
        functools.partial(exchange_kernel, planes, seats),
        out_shape=jax.ShapeDtypeStruct((rows, width), jnp.bfloat16),
        in_specs=[pl.BlockSpec(memory_space=pltpu.VMEM)] * 4,
        out_specs=pl.BlockSpec(memory_space=pltpu.VMEM),
        scratch_shapes=[
            pltpu.VMEM((blocks * rows, head_size), jnp.bfloat16),
            pltpu.VMEM((blocks * rows, 2 * head_size), jnp.bfloat16),
            pltpu.VMEM((planes, rows, head_size), jnp.bfloat16),
            pltpu.VMEM((planes, rows, head_size), jnp.bfloat16),
            pltpu.VMEM((planes, rows, 2 * head_size), jnp.float32),
            pltpu.VMEM((planes, rows, LANES), jnp.float32),
            dma((3, planes)), dma((3, planes)),
            dma((2, planes)), dma((2, planes)),
            dma((2, planes)), dma((2, planes)),
            dma((2, planes)), dma((2, planes)),
            dma((planes,)), dma((planes,)),
        ],
        compiler_params=pltpu.CompilerParams(
            collective_id=0, has_side_effects=True, vmem_limit_bytes=48 * 2**20
        ),
        cost_estimate=pl.CostEstimate(
            flops=4 * pairs * rows * rows * head_size,
            bytes_accessed=2 * 4 * rows * width,
            transcendentals=pairs * rows * rows,
        ),
    )(query, keys, values, log_gates)


def ring_attend(query, keys, values, log_gates):
    tok_rows = query.shape[0]
    heads = log_gates.shape[0]
    head_size = query.shape[1] // heads
    devices = lax.axis_size("sp")
    side = 1
    while (2 * side) ** 2 <= devices and devices % (2 * side) == 0:
        side = 2 * side
    planes = devices // side
    sequence_index = lax.axis_index("sp")
    plane = sequence_index // side
    seat = sequence_index % side
    pair = jnp.concatenate([keys, values], axis=1)
    pairs = [pair]
    for _ in range(1, planes):
        pairs.append(passed_along(pairs[-1], "sp", side))
    queries = jnp.stack([query] + [swapped(query, "sp", g) for g in range(1, side)])
    seats = seat ^ jnp.arange(side, dtype=jnp.int32)
    starts = jnp.stack(
        [
            lax.dynamic_slice_in_dim(log_gates, (plane * side + (seat ^ g)) * tok_rows, 1, 1)[:, 0]
            for g in range(side)
        ]
    ).reshape(-1)
    state = None
    for k in range(planes):
        source = jnp.maximum(sequence_index - k * side, seat)
        gates = lax.dynamic_slice_in_dim(log_gates, source * tok_rows, tok_rows, 1)
        if k == 0:
            mode = (seats > seat).astype(jnp.int32)
        else:
            mode = jnp.full((side,), plane >= k, jnp.int32)
        state = attend_step(
            mode, starts, queries, pairs[k], gates, state, k == planes - 1, head_size
        )
    partial, level = state
    level = level[:, :, :heads]
    shares = [partial[0]] + [swapped(partial[g], "sp", g) for g in range(1, side)]
    tall = jnp.transpose(level, (0, 2, 1))
    levels = jnp.stack([tall[0]] + [swapped(tall[g], "sp", g) for g in range(1, side)])
    portion = jnp.exp2(levels - jnp.max(levels, axis=0, keepdims=True))
    portion = portion / jnp.sum(portion, axis=0, keepdims=True)
    portion = jnp.transpose(portion, (0, 2, 1))
    attended = 0.0
    for g in range(side):
        attended = attended + shares[g].astype(jnp.float32) * jnp.repeat(portion[g], head_size, axis=1)
    return attended.astype(jnp.bfloat16)


def gathered(block, axis):
    if lax.axis_size(axis) != 2:
        return lax.all_gather(block, axis, axis=1, tiled=True)
    other = swapped(block, axis, 1)
    lower = lax.axis_index(axis) == 0
    return jnp.concatenate([jnp.where(lower, block, other), jnp.where(lower, other, block)], axis=1)


def body(
    tokens,
    input_gain,
    query_weight,
    key_weight,
    value_weight,
    pool_in_weight,
    log_gates,
    pool_weight,
    pool_scale,
    attention_out,
    pooling_out,
    final_gain,
):
    tok_rows = tokens.shape[0]
    width = query_weight.shape[0]
    groups = pool_weight.shape[0]
    head_size = pool_weight.shape[1]
    heads = log_gates.shape[0]
    pool_width = pool_in_weight.shape[1]
    devices = lax.axis_size("sp")
    shards = lax.axis_size("tp")
    sequence_index = lax.axis_index("sp")
    first_row = sequence_index * tok_rows

    part = gathered(tokens, "tp")
    gain_part = gathered(input_gain.reshape(1, -1), "tp")
    widened = part.astype(jnp.float32)
    scaled = (widened * gain_part.astype(jnp.float32)).astype(jnp.bfloat16)

    def product(weight):
        return jnp.dot(scaled, weight, preferred_element_type=jnp.float32)

    inverse = lax.rsqrt(jnp.sum(widened * widened, axis=1) / width + epsilon)[:, None]
    keys = (product(key_weight) * inverse).astype(jnp.bfloat16)
    values = (product(value_weight) * inverse).astype(jnp.bfloat16)
    query = (product(query_weight) * (inverse * (LOG2E * head_size ** (-0.5)))).astype(jnp.bfloat16)
    pool_input = (product(pool_in_weight) * inverse).astype(jnp.bfloat16)
    rim = passed_along(pool_input[tok_rows - (WINDOW_MAX - 1) :], "sp", 1)

    spread = heads > 1 and devices == 4 * heads
    if spread:
        attended = exchange_attend(query, keys, values, log_gates)
    else:
        attended = ring_attend(query, keys, values, log_gates)

    extended = jnp.concatenate([rim, pool_input], axis=0).astype(jnp.float32)
    column = jnp.arange(pool_width, dtype=jnp.int32)
    group_number = lax.axis_index("tp") * groups + column // head_size
    window = jnp.left_shift(jnp.full((pool_width,), 2, jnp.int32), group_number % 4)
    sums = extended
    span = 1
    chosen = jnp.zeros((tok_rows, pool_width), jnp.float32)
    for _ in range(4):
        sums = sums[span:] + sums[:-span]
        span = span * 2
        offset_rows = WINDOW_MAX - span
        chosen = jnp.where(window[None, :] == span, sums[offset_rows : offset_rows + tok_rows], chosen)
    element_locations = first_row + jnp.arange(tok_rows, dtype=jnp.int32)
    counts = jnp.minimum(window[None, :], element_locations[:, None] + 1).astype(jnp.float32)
    departure = (chosen / counts - pool_input.astype(jnp.float32)).astype(jnp.bfloat16)
    mapped = jnp.concatenate(
        [
            jnp.dot(
                departure[:, g * head_size : (g + 1) * head_size],
                pool_weight[g],
                preferred_element_type=jnp.float32,
            )
            for g in range(groups)
        ],
        axis=1,
    )
    pooled = (mapped * pool_scale).astype(jnp.bfloat16)
    pooled_part = jnp.dot(pooled, pooling_out, preferred_element_type=jnp.float32)
    whole = jnp.dot(attended, attention_out, preferred_element_type=jnp.float32) + pooled_part
    if shards == 2:
        half = width // 2
        lower = lax.axis_index("tp") == 0
        sent = jnp.where(lower, whole[:, half:], whole[:, :half]).astype(jnp.bfloat16)
        kept = jnp.where(lower, whole[:, :half], whole[:, half:])
        mixed = kept + swapped(sent, "tp", 1).astype(jnp.float32)
        squares = jnp.sum(mixed * mixed, axis=1)
        squares = squares + swapped(squares, "tp", 1)
    else:
        mixed = lax.psum_scatter(
            whole.astype(jnp.bfloat16), "tp", scatter_dimension=1, tiled=True
        ).astype(jnp.float32)
        squares = lax.psum(jnp.sum(mixed * mixed, axis=1), "tp")
    out_inverse = lax.rsqrt(squares / width + epsilon)
    return (mixed * out_inverse[:, None] * final_gain[None, :]).astype(jnp.bfloat16)


def solution(mesh):
    return jax.shard_map(
        body,
        mesh=mesh,
        in_specs=(
            P("sp", "tp"),
            P("tp"),
            P(None, "tp"),
            P(None, "tp"),
            P(None, "tp"),
            P(None, "tp"),
            P("tp", None),
            P("tp", None, None),
            P("tp"),
            P("tp", None),
            P("tp", None),
            P("tp"),
        ),
        out_specs=P("sp", "tp"),
        check_vma=False,
    )
```

profile of v0, /device:TPU:0, one launch (start us, length us, event | category | flops | bytes accessed | tf_op | source)
XLA Modules:
  0.0 98.6 jit_solution(4830824421250746105)
XLA Ops:
  0.0 0.0 copy-start
  0.0 0.5 collective-permute-start
  0.5 0.8 reshape.81
  1.3 0.0 collective-permute-start.1
  1.4 1.6 %collective-permute-done.1 = bf16[1,1024]{1,0:T(2,128)(2,1)S(1)} collective-permute-done((bf16[1,1024]{1,0:T(2,128)(2,1)S(1)}, bf16[1,1024]{1,0:T(2,128)(2,1)S(1)}, u32[]{:S(2)}, u32[]{:S(2)}) %collective-permute-start.1) | collective-permute-done | bytes 2080 | tf_op jit(solution)/shard_map/ppermute | solution.py:26
  3.0 0.7 fusion.31
  3.7 0.0 collective-permute-done
  3.7 1.4 %broadcast_select_fusion.1 = (bf16[512,1024]{1,0:T(8,128)(2,1)S(1)}, bf16[512,1024]{1,0:T(8,128)(2,1)S(1)}) fusion(bf16[512,1024]{1,0:T(8,128)(2,1)} %param.12, bf16[512,1024]{1,0:T(8,128)(2,1)S(1)} %collective-permute-done, pred[]{:T(512)S(6)} %eq.47), kind=kLoop, calls=%fused_computation.32 | loop fusion | flops 1048576 | bytes 4194305 | tf_op jit(solution)/shard_map/jit(_where)/select_n | solution.py:461
  5.1 0.0 copy-start.6
  5.1 0.5 fusion.1
  5.6 1.1 %copy-done.6 = bf16[2048,512]{1,0:T(8,128)(2,1)S(1)} copy-done((bf16[2048,512]{1,0:T(8,128)(2,1)S(1)}, bf16[2048,512]{1,0:T(8,128)(2,1)}, u32[]{:S(2)}) %copy-start.6) | copy-done | bytes 2097176
  6.7 0.0 copy-start.7
  6.7 1.3 %fusion.5 = bf16[512,512]{1,0:T(8,128)(2,1)S(1)} fusion(bf16[2048,512]{1,0:T(8,128)(2,1)S(1)} %copy-done.6, f32[512]{0:T(512)S(1)} %get-tuple-element.9, f32[2048]{0:T(1024)S(1)} %maximum_convert_fusion.1, bf16[512,1024]{1,0:T(8,128)(2,1)S(1)} %get-tuple-element.8, bf16[512,1024]{1,0:T(8,128)(2,1)S(1)} %get-tuple-element.7), kind=kOutput, calls=%fused_computation.17 | convolution fusion | flops 1080557568 | bytes 4728832 | tf_op jit(solution)/shard_map/dot_general | solution.py:495
  8.0 0.0 copy-start.8
  8.0 4.9 %collective-permute-start.2 = (bf16[15,512]{1,0:T(8,128)(2,1)S(1)}, bf16[15,512]{1,0:T(8,128)(2,1)S(1)}, u32[]{:S(2)}, u32[]{:S(2)}) collective-permute-start(bf16[15,512]{1,0:T(8,128)(2,1)S(1)} %slice.87), channel_id=1, source_target_pairs={{0,2},{2,4},{4,6},{6,8},{8,10},{10,12},{12,14},{14,16},{16,18},{18... | collective-permute-start | bytes 46088 | tf_op jit(solution)/shard_map/ppermute | solution.py:22
  12.9 0.0 copy-done.7
  12.9 1.2 %fusion.3.k_ref = bf16[512,512]{1,0:T(8,128)(2,1)S(1)} fusion(bf16[2048,512]{1,0:T(8,128)(2,1)S(1)} %copy-done.7, f32[512]{0:T(512)S(1)} %get-tuple-element.9, f32[2048]{0:T(1024)S(1)} %maximum_convert_fusion.1, bf16[512,1024]{1,0:T(8,128)(2,1)S(1)} %get-tuple-element.8, bf16[512,1024]{1,0:T(8,128)(2,1)S(1)} %get-tuple-element.7), kind=kOutput, calls=%fused_computation.15 | convolution fusion | flops 1080557568 | bytes 4728832 | tf_op jit(solution)/shard_map/dot_general | solution.py:495
  14.1 0.0 copy-done.8
  14.1 0.0 copy-start.9
  14.2 1.3 %fusion.4.v_ref = bf16[512,512]{1,0:T(8,128)(2,1)S(1)} fusion(bf16[2048,512]{1,0:T(8,128)(2,1)S(1)} %copy-done.8, f32[512]{0:T(512)S(1)} %get-tuple-element.9, f32[2048]{0:T(1024)S(1)} %maximum_convert_fusion.1, bf16[512,1024]{1,0:T(8,128)(2,1)S(1)} %get-tuple-element.8, bf16[512,1024]{1,0:T(8,128)(2,1)S(1)} %get-tuple-element.7), kind=kOutput, calls=%fused_computation.16 | convolution fusion | flops 1080557568 | bytes 4728832 | tf_op jit(solution)/shard_map/dot_general | solution.py:495
  15.4 0.3 copy-done.9
  15.7 0.0 copy-start.1
  15.7 1.3 %fusion.2.q_ref = bf16[512,512]{1,0:T(8,128)(2,1)S(1)} fusion(bf16[2048,512]{1,0:T(8,128)(2,1)S(1)} %copy-done.9, f32[512]{0:T(512)S(1)} %get-tuple-element.10, f32[2048]{0:T(1024)S(1)} %maximum_convert_fusion.1, bf16[512,1024]{1,0:T(8,128)(2,1)S(1)} %get-tuple-element.8, bf16[512,1024]{1,0:T(8,128)(2,1)S(1)} %get-tuple-element.7), kind=kOutput, calls=%fused_computation.14 | convolution fusion | flops 1080557568 | bytes 4728832 | tf_op jit(solution)/shard_map/dot_general | solution.py:495
  17.0 0.0 copy-done.1
  17.0 70.8 %shard_map.118 = bf16[512,512]{1,0:T(8,128)(2,1)S(1)} custom-call(bf16[512,512]{1,0:T(8,128)(2,1)S(1)} %fusion.2.q_ref, bf16[512,512]{1,0:T(8,128)(2,1)S(1)} %fusion.3.k_ref, bf16[512,512]{1,0:T(8,128)(2,1)S(1)} %fusion.4.v_ref, f32[4,8192]{1,0:T(4,128)S(1)} %copy-done.1), custom_call_target="tpu_custom_call" | custom-call | flops 18253611008 | bytes 2097152 | tf_op jit(solution)/shard_map/pallas_call | solution.py:378
  87.8 0.0 copy-done
  87.8 1.3 %fusion.44 = f32[512,2048]{1,0:T(8,128)S(1)} fusion(bf16[512,512]{1,0:T(8,128)(2,1)S(1)} %shard_map.118, bf16[512,2048]{1,0:T(8,128)(2,1)S(1)} %copy-done), kind=kOutput, calls=%fused_computation.78 | convolution fusion | flops 1073741824 | bytes 6815744 | tf_op jit(solution)/shard_map/dot_general | solution.py:538
  89.1 0.0 collective-permute-done.2
  89.1 0.1 maximum_convert_fusion
  89.3 0.1 slice_add_fusion.1
  89.4 0.1 slice_add_fusion
  89.6 0.1 slice_add_fusion.2
  89.7 0.0 copy-start.3
  89.7 0.0 copy-start.2
  89.7 0.0 copy-start.4
  89.8 0.6 fusion.12
  90.4 0.2 copy-done.3
  90.6 0.2 fusion.15
  90.8 0.2 fusion.17
  91.0 0.2 fusion.19
  91.1 0.2 fusion.21
  91.3 0.1 copy-done.2
  91.4 0.0 copy-done.4
  91.4 1.3 %convolution_add_fusion = f32[512,2048]{1,0:T(8,128)S(1)} fusion(f32[512,2048]{1,0:T(8,128)S(1)} %fusion.44, bf16[512,2048]{1,0:T(8,128)(2,1)S(1)} %copy-done.2, f32[512,128]{1,0:T(8,128)S(1)} %fusion.15, f32[512,128]{1,0:T(8,128)S(1)} %fusion.17, f32[512,128]{1,0:T(8,128)S(1)} %fusion.19, f32[512,128]{1,0:T(8,128)S(1)} %fusion.21, f32[512]{0:T(512)S(1)} %copy-done.4), kind=kOutput, calls=%fused_computation.4 | convolution fusion | flops 1076101120 | bytes 11536384 | tf_op jit(solution)/shard_map/dot_general | solution.py:537
  92.7 0.2 select_convert_fusion
  92.9 0.0 copy-start.5
  92.9 0.1 collective-permute-start.3
  93.0 2.6 %collective-permute-done.3 = bf16[512,1024]{1,0:T(8,128)(2,1)S(1)} collective-permute-done((bf16[512,1024]{1,0:T(8,128)(2,1)S(1)}, bf16[512,1024]{1,0:T(8,128)(2,1)S(1)}, u32[]{:S(2)}, u32[]{:S(2)}) %collective-permute-start.3) | collective-permute-done | bytes 1048608 | tf_op jit(solution)/shard_map/ppermute | solution.py:26
  95.6 0.4 multiply_reduce_fusion
  96.0 0.2 collective-permute-start.4
  96.2 1.0 %collective-permute-done.4 = f32[512]{0:T(512)S(1)} collective-permute-done((f32[512]{0:T(512)S(1)}, f32[512]{0:T(512)S(1)}, u32[]{:S(2)}, u32[]{:S(2)}) %collective-permute-start.4) | collective-permute-done | bytes 2080 | tf_op jit(solution)/shard_map/ppermute | solution.py:26
  97.2 0.0 copy-done.5
  97.3 1.4 %multiply_convert_fusion = bf16[512,1024]{1,0:T(8,128)(2,1)} fusion(f32[1024]{0:T(1024)S(1)} %copy-done.5, f32[512]{0:T(512)S(1)} %add_rsqrt_fusion, bf16[512,1024]{1,0:T(8,128)(2,1)S(1)} %collective-permute-done.3, f32[512,2048]{1,0:T(8,128)S(1)} %convolution_add_fusion, pred[]{:T(512)S(6)} %eq.47), kind=kLoop, calls=%fused_computation.6 | loop fusion | flops 3145728 | bytes 6297601 | tf_op jit(solution)/shard_map/convert_element_type | solution.py:553
  (7 shorter events, 0.1 us)
Async XLA Ops:
  0.0 87.8 %copy-start = (bf16[512,2048]{1,0:T(8,128)(2,1)S(1)}, bf16[512,2048]{1,0:T(8,128)(2,1)}, u32[]{:S(2)}) copy-start(bf16[512,2048]{1,0:T(8,128)(2,1)} %param.21) | copy-start | bytes 6291460
  0.0 3.7 %collective-permute-start = (bf16[512,1024]{1,0:T(8,128)(2,1)}, bf16[512,1024]{1,0:T(8,128)(2,1)S(1)}, u32[]{:S(2)}, u32[]{:S(2)}) collective-permute-start(bf16[512,1024]{1,0:T(8,128)(2,1)} %param.12), channel_id=1, source_target_pairs={{0,1},{1,0},{2,3},{3,2},{4,5},{5,4},{6,7},{7,6},{8,9},{9,8},{10,11... | collective-permute-start | bytes 3145736 | tf_op jit(solution)/shard_map/ppermute | solution.py:26
  1.3 1.7 %collective-permute-start.1 = (bf16[1,1024]{1,0:T(2,128)(2,1)S(1)}, bf16[1,1024]{1,0:T(2,128)(2,1)S(1)}, u32[]{:S(2)}, u32[]{:S(2)}) collective-permute-start(bf16[1,1024]{1,0:T(2,128)(2,1)S(1)} %reshape.81), channel_id=1, source_target_pairs={{0,1},{1,0},{2,3},{3,2},{4,5},{5,4},{6,7},{7,6},{8,9},{9,8},{10,11... | collective-permute-start | bytes 6152 | tf_op jit(solution)/shard_map/ppermute | solution.py:26
  5.1 1.6 %copy-start.6 = (bf16[2048,512]{1,0:T(8,128)(2,1)S(1)}, bf16[2048,512]{1,0:T(8,128)(2,1)}, u32[]{:S(2)}) copy-start(bf16[2048,512]{1,0:T(8,128)(2,1)} %param.17) | copy-start | bytes 6291460
  6.7 6.2 %copy-start.7 = (bf16[2048,512]{1,0:T(8,128)(2,1)S(1)}, bf16[2048,512]{1,0:T(8,128)(2,1)}, u32[]{:S(2)}) copy-start(bf16[2048,512]{1,0:T(8,128)(2,1)} %param.15) | copy-start | bytes 6291460
  8.0 6.2 %copy-start.8 = (bf16[2048,512]{1,0:T(8,128)(2,1)S(1)}, bf16[2048,512]{1,0:T(8,128)(2,1)}, u32[]{:S(2)}) copy-start(bf16[2048,512]{1,0:T(8,128)(2,1)} %param.16) | copy-start | bytes 6291460
  8.0 81.1 %collective-permute-start.2 = (bf16[15,512]{1,0:T(8,128)(2,1)S(1)}, bf16[15,512]{1,0:T(8,128)(2,1)S(1)}, u32[]{:S(2)}, u32[]{:S(2)}) collective-permute-start(bf16[15,512]{1,0:T(8,128)(2,1)S(1)} %slice.87), channel_id=1, source_target_pairs={{0,2},{2,4},{4,6},{6,8},{8,10},{10,12},{12,14},{14,16},{16,18},{18... | collective-permute-start | bytes 46088 | tf_op jit(solution)/shard_map/ppermute | solution.py:22
  14.1 1.6 %copy-start.9 = (bf16[2048,512]{1,0:T(8,128)(2,1)S(1)}, bf16[2048,512]{1,0:T(8,128)(2,1)}, u32[]{:S(2)}) copy-start(bf16[2048,512]{1,0:T(8,128)(2,1)} %param.14) | copy-start | bytes 6291460
  15.7 1.3 %copy-start.1 = (f32[4,8192]{1,0:T(4,128)S(1)}, f32[4,8192]{1,0:T(4,128)}, u32[]{:S(2)}) copy-start(f32[4,8192]{1,0:T(4,128)} %gate_ref.1) | copy-start | bytes 393220
  89.7 0.9 copy-start.3
  89.7 1.7 %copy-start.2 = (bf16[512,2048]{1,0:T(8,128)(2,1)S(1)}, bf16[512,2048]{1,0:T(8,128)(2,1)}, u32[]{:S(2)}) copy-start(bf16[512,2048]{1,0:T(8,128)(2,1)} %param.22) | copy-start | bytes 6291460
  89.7 1.7 %copy-start.4 = (f32[512]{0:T(512)S(1)}, f32[512]{0:T(512)}, u32[]{:S(2)}) copy-start(f32[512]{0:T(512)} %param.20) | copy-start | bytes 6148
  92.9 4.4 %copy-start.5 = (f32[1024]{0:T(1024)S(1)}, f32[1024]{0:T(1024)}, u32[]{:S(2)}) copy-start(f32[1024]{0:T(1024)} %param.23) | copy-start | bytes 12292
  92.9 2.7 %collective-permute-start.3 = (bf16[512,1024]{1,0:T(8,128)(2,1)S(1)}, bf16[512,1024]{1,0:T(8,128)(2,1)S(1)}, u32[]{:S(2)}, u32[]{:S(2)}) collective-permute-start(bf16[512,1024]{1,0:T(8,128)(2,1)S(1)} %select_convert_fusion), channel_id=1, source_target_pairs={{0,1},{1,0},{2,3},{3,2},{4,5},{5,4},{6,7},{7,6},{8,9},{9,8},{10,11... | collective-permute-start | bytes 3145736 | tf_op jit(solution)/shard_map/ppermute | solution.py:26
  96.0 1.2 %collective-permute-start.4 = (f32[512]{0:T(512)S(1)}, f32[512]{0:T(512)S(1)}, u32[]{:S(2)}, u32[]{:S(2)}) collective-permute-start(f32[512]{0:T(512)S(1)} %multiply_reduce_fusion), channel_id=1, source_target_pairs={{0,1},{1,0},{2,3},{3,2},{4,5},{5,4},{6,7},{7,6},{8,9},{9,8},{10,11... | collective-permute-start | bytes 6152 | tf_op jit(solution)/shard_map/ppermute | solution.py:26
where the time goes:
time: 98.9 us; the launch traced here: 98.6 us
  Pallas kernels  70.8 us (72%)
  matrix products  8.2 us (8%)
  other arithmetic  5.82 us (6%)
  starting transfers between devices  5.66 us (6%)
  waiting for transfers between devices  5.28 us (5%)
  local copies, waits for them, and re-layouts  2.6 us (3%)
    pallas_call x1, Pallas kernels, exchange_attend(): pl.pallas_call(functools.partial(exchange_kernel, planes, seats), out_sha...  70.8 us
    ppermute x4, waiting for transfers between devices, swapped(): lax.ppermute(block, axis, [(i, i ^ offset) for i in range(lax.axis_size(a...  5.28 us
    dot_general x4, matrix products, product(): return jnp.dot(scaled, weight, preferred_element_type=jnp.float32)  5.02 us
    ppermute x1, starting transfers between devices, passed_along(): return lax.ppermute(block, axis, route)  4.87 us
    select_n x2, other arithmetic, gathered(): jnp.where(lower, block, other)  2.08 us
  transfers between devices with their start and end apart: 5, of which 3 were waited for; matrix products, arithmetic and copies ran while one was open for 7% of the time, Pallas kernels for 72%

commit v1 on v0

--- a/solution.py
+++ b/solution.py
@@ -151,21 +151,45 @@
 SUB_ROWS = 128
 
 
-def exchange_kernel(
-    planes, seats, q_ref, k_ref, v_ref, gate_ref, out_ref,
-    keys, values, queries, results, acc, high,
+def layer_kernel(
+    tokens_ref, gain_ref, query_weight, key_weight, value_weight, pool_in_weight, gate_ref,
+    pool_weight_ref, pool_scale_ref, attention_out, pooling_out, final_gain_ref, out_ref,
+    weights, outs, halves, norms, inverse, made, rim, pool_input, extended, pooled, whole, sent, got, row_sums,
+    keys, values, queries, results, attended, acc, high,
+    w_sem, c_send, c_recv, e_send, e_recv, rim_send, rim_recv,
     z_send, z_recv, x_send, x_recv, y_send, y_recv, r_send, r_recv, o_send, o_recv,
 ):
-    rows, head_size = queries.shape[1:]
-    me = lax.axis_index("sp")
+    planes, rows, head_size = queries.shape
+    width = 2 * halves.shape[2]
+    half = width // 2
+    inner = made.shape[2]
+    groups = pool_weight_ref.shape[0]
+    me, core = lax.axis_index("sp"), lax.axis_index("tp")
+    devices = lax.axis_size("sp")
+    seats = devices // planes
     plane, seat = me // seats, me % seats
     across = seat + 1 - 2 * (seat % 2)
     along = seat + 2 - 4 * (seat // 2)
     far = 3 - seat
+    reach = planes - 1
+
+    loads = [
+        pltpu.make_async_copy(source, target, w_sem.at[n])
+        for n, (source, target) in enumerate(
+            [
+                (key_weight, weights.at[0]), (value_weight, weights.at[1]), (query_weight, weights.at[2]),
+                (pool_in_weight, weights.at[3]), (pooling_out, outs.at[0]), (attention_out, outs.at[1]),
+            ]
+        )
+    ]
+    for load in loads:
+        load.start()
 
     def device(p, s):
         return {"sp": p * seats + s}
 
+    sibling = {"tp": 1 - core}
+
     def block_rows(p, s):
         return pl.ds(pl.multiple_of((p * seats + s) * rows, rows), rows)
 
@@ -178,93 +202,153 @@
     def value_at(p, s):
         return values.at[block_rows(p, s), pl.ds(0, head_size)]
 
-    def copy(source, target, send, recv, p, s):
+    def copy(source, target, send, recv, to):
         return pltpu.make_async_remote_copy(
-            src_ref=source, dst_ref=target, send_sem=send, recv_sem=recv,
-            device_id=device(p, s), device_id_type=MESH,
-        )
+            src_ref=source, dst_ref=target, send_sem=send, recv_sem=recv, device_id=to, device_id_type=MESH
+        )
+
+    def arrival(target, recv):
+        copy(target, target, z_send.at[0, 0], recv, sibling).wait_recv()
 
     barrier = pltpu.get_barrier_semaphore()
+
+    def greet(to):
+        pl.semaphore_signal(barrier, inc=1, device_id=to, device_id_type=MESH)
+
     for d in range(1, planes):
-        pl.semaphore_signal(barrier, inc=1, device_id=device((plane + d) % planes, seat), device_id_type=MESH)
-    for s in (across, along):
-        pl.semaphore_signal(barrier, inc=1, device_id=device(plane, s), device_id_type=MESH)
-    pl.semaphore_wait(barrier, planes + 1)
-
-    def from_plane(d):
-        return (plane + planes - d) % planes
-
-    def query_copy(d):
-        to = (plane + d) % planes
-        return copy(q_ref.at[:, columns(to)], queries.at[plane], z_send.at[0, d], z_recv.at[0, d], to, seat)
-
-    def pair_copies(d):
-        to = (plane + d) % planes
+        greet(device((plane + d) % planes, seat))
+    greet(device(plane, across))
+    greet(device(plane, along))
+    greet(sibling)
+    greet({"sp": (me + 1) % devices})
+    greet({"sp": (me + devices - 1) % devices})
+
+    def scale_rows(n, carry):
+        at = pl.ds(pl.multiple_of(n * SUB_ROWS, SUB_ROWS), SUB_ROWS)
+        widened = tokens_ref[at, :].astype(jnp.float32)
+        halves[core, at, :] = (widened * gain_ref[...].astype(jnp.float32)).astype(jnp.bfloat16)
+        square = widened * widened
+        norms[core, at, :] = functools.reduce(
+            jnp.add, [square[:, c : c + LANES] for c in range(0, half, LANES)]
+        )
+        return carry
+
+    lax.fori_loop(0, rows // SUB_ROWS, scale_rows, 0)
+    pl.semaphore_wait(barrier, planes + 4)
+
+    swaps = (
+        copy(halves.at[core], halves.at[core], c_send.at[0], c_recv.at[0], sibling),
+        copy(norms.at[core], norms.at[core], c_send.at[1], c_recv.at[1], sibling),
+    )
+    for c in swaps:
+        c.start()
+    values[:, head_size:] = jnp.ones((values.shape[0], head_size), values.dtype)
+    arrival(norms.at[1 - core], c_recv.at[1])
+    total = jnp.sum(norms[0] + norms[1], axis=1, keepdims=True)
+    inverse[...] = jnp.broadcast_to(lax.rsqrt(total / width + epsilon), inverse.shape)
+    arrival(halves.at[1 - core], c_recv.at[0])
+
+    def project(n, factor, store):
+        loads[n].wait()
+
+        def one(c, carry):
+            at = pl.ds(pl.multiple_of(c * 2 * LANES, 2 * LANES), 2 * LANES)
+            r = jnp.dot(halves[0], weights[n, :half, at], preferred_element_type=jnp.float32)
+            r = r + jnp.dot(halves[1], weights[n, half:, at], preferred_element_type=jnp.float32)
+            f = inverse[...] * factor
+            store(at, (r * jnp.concatenate([f, f], axis=1)).astype(jnp.bfloat16))
+            return carry
+
+        lax.fori_loop(0, inner // (2 * LANES), one, 0)
+
+    def keep(n):
+        def store(at, value):
+            made[n, :, at] = value
+
+        return store
+
+    def at_reach(step):
+        other = plane + (1 + step // 2) * (1 - 2 * (step % 2))
+        return other, (other >= 0) & (other < planes)
+
+    def query_copy(to):
+        return copy(
+            made.at[2, :, columns(to)], queries.at[plane], z_send.at[2, to], z_recv.at[2, plane], device(to, seat)
+        )
+
+    def tensor_copy(n, to):
+        target = (key_at, value_at)[n](plane, seat)
+        return copy(made.at[n, :, columns(to)], target, z_send.at[n, to], z_recv.at[n, plane], device(to, seat))
+
+    def spread(n, p, own):
+        target = (key_at, value_at)[n](p, seat)
+        source = made.at[n, :, columns(plane)] if own else target
         return (
-            copy(k_ref.at[:, columns(to)], key_at(plane, seat), z_send.at[1, d], z_recv.at[1, d], to, seat),
-            copy(v_ref.at[:, columns(to)], value_at(plane, seat), z_send.at[2, d], z_recv.at[2, d], to, seat),
-        )
-
-    def spread(d, own):
-        p = from_plane(d)
-        k = k_ref.at[:, columns(plane)] if own else key_at(p, seat)
-        v = v_ref.at[:, columns(plane)] if own else value_at(p, seat)
+            copy(source, target, x_send.at[n, p], x_recv.at[n, p], device(plane, across)),
+            copy(source, target, y_send.at[n, p], y_recv.at[n, p], device(plane, along)),
+        )
+
+    def relays(p):
+        k, v = key_at(p, across), value_at(p, along)
         return (
-            copy(k, key_at(p, seat), x_send.at[0, d], x_recv.at[0, d], plane, across),
-            copy(v, value_at(p, seat), y_send.at[1, d], y_recv.at[1, d], plane, along),
-            copy(v, value_at(p, seat), x_send.at[1, d], x_recv.at[1, d], plane, across),
-            copy(k, key_at(p, seat), y_send.at[0, d], y_recv.at[0, d], plane, along),
-        )
-
-    def relays(d):
-        p = from_plane(d)
-        return (
-            copy(key_at(p, across), key_at(p, across), r_send.at[0, d], r_recv.at[0, d], plane, along),
-            copy(value_at(p, along), value_at(p, along), r_send.at[1, d], r_recv.at[1, d], plane, across),
-        )
-
-    def arrival(target, recv):
-        pltpu.make_async_remote_copy(
-            src_ref=target, dst_ref=target, send_sem=z_send.at[0, 0], recv_sem=recv,
-            device_id=device(plane, across), device_id_type=MESH,
-        ).wait_recv()
-
-    for d in range(1, planes):
-        query_copy(d).start()
-    for d in range(1, planes):
-        for c in pair_copies(d):
+            copy(k, k, r_send.at[0, p], r_recv.at[0, p], device(plane, along)),
+            copy(v, v, r_send.at[1, p], r_recv.at[1, p], device(plane, across)),
+        )
+
+    def each(steps, action):
+        for step in steps:
+            other, valid = at_reach(step)
+            pl.when(valid)(functools.partial(action, other))
+
+    def start_all(copies):
+        for c in copies:
             c.start()
-    for c in spread(0, True):
-        c.start()
-
-    values[:, head_size:] = jnp.ones((values.shape[0], head_size), values.dtype)
-    keys[block_rows(plane, seat), :] = k_ref[:, columns(plane)]
-    values[block_rows(plane, seat), :head_size] = v_ref[:, columns(plane)]
-    queries[plane] = q_ref[:, columns(plane)]
+
+    def send_pair(to):
+        start_all((tensor_copy(0, to), tensor_copy(1, to)))
+
+    project(0, 1.0, keep(0))
+    each(range(2), lambda to: tensor_copy(0, to).start())
+    start_all(spread(0, plane, True))
+    project(1, 1.0, keep(1))
+    each(range(2), lambda to: tensor_copy(1, to).start())
+    start_all(spread(1, plane, True))
+    each(range(2, 2 * reach), send_pair)
+    project(2, LOG2E * head_size ** (-0.5), keep(2))
+    each(reversed(range(2 * reach)), lambda to: query_copy(to).start())
+
+    keys[block_rows(plane, seat), :] = made[0, :, columns(plane)]
+    values[block_rows(plane, seat), :head_size] = made[1, :, columns(plane)]
+    queries[plane] = made[2, :, columns(plane)]
     acc[...] = jnp.zeros_like(acc)
     high[...] = jnp.full_like(high, very_low)
 
-    def forward(d):
-        p = from_plane(d)
-        arrival(key_at(p, seat), z_recv.at[1, d])
-        arrival(value_at(p, seat), z_recv.at[2, d])
-        for c in spread(d, False):
-            c.start()
-
-    def relay(d):
-        p = from_plane(d)
-        to_along, to_across = relays(d)
-        arrival(key_at(p, across), x_recv.at[0, d])
+    def keep_pool(at, value):
+        pool_input[:, at] = value
+
+    project(3, 1.0, keep_pool)
+    rim_copy = copy(
+        pool_input.at[pl.ds(rows - WINDOW_MAX, WINDOW_MAX), :], rim, rim_send, rim_recv, {"sp": (me + 1) % devices}
+    )
+    rim_copy.start()
+
+    def forward(p):
+        for n in range(2):
+            arrival((key_at, value_at)[n](p, seat), z_recv.at[n, p])
+            start_all(spread(n, p, False))
+
+    def relay(p):
+        to_along, to_across = relays(p)
+        arrival(key_at(p, across), x_recv.at[0, p])
         to_along.start()
-        arrival(value_at(p, along), y_recv.at[1, d])
+        arrival(value_at(p, along), y_recv.at[1, p])
         to_across.start()
 
-    def settle(d):
-        p = from_plane(d)
-        arrival(value_at(p, across), x_recv.at[1, d])
-        arrival(key_at(p, along), y_recv.at[0, d])
-        arrival(key_at(p, far), r_recv.at[0, d])
-        arrival(value_at(p, far), r_recv.at[1, d])
+    def settle(p):
+        arrival(value_at(p, across), x_recv.at[1, p])
+        arrival(key_at(p, along), y_recv.at[0, p])
+        arrival(key_at(p, far), r_recv.at[0, p])
+        arrival(value_at(p, far), r_recv.at[1, p])
 
     span = seats * rows
 
@@ -299,94 +383,189 @@
             acc[i, at, :] = acc[i, at, :] * jnp.concatenate([factor, factor], axis=1) + summed
             high[i, at, :] = new
 
-    def finished(t):
-        to = (plane + t) % planes
-        return copy(results.at[to], out_ref.at[:, columns(plane)], o_send.at[t], o_recv.at[t], to, seat)
-
-    relay(0)
-    for d in range(1, planes):
-        p = from_plane(d)
-        arrival(queries.at[p], z_recv.at[0, d])
-
-    def step(d, carry):
-        @pl.when(d > 0)
+    def finished(to):
+        return copy(
+            results.at[to], attended.at[:, columns(plane)], o_send.at[to], o_recv.at[plane], device(to, seat)
+        )
+
+    def own_update(p):
+        settle(p)
+
+        @pl.when(p < plane)
         def _():
-            relay(d)
-
-        @pl.when(d < planes - 1)
+            update(plane, p, False)
+
+        @pl.when(p == plane)
         def _():
-            forward(d + 1)
-
-        settle(d)
-        p = from_plane(d)
-
-        def one(t, carry):
-            i = (plane + t) % planes
-
-            @pl.when(i > p)
-            def _():
+            update(plane, p, True)
+
+    def gather(step, carry):
+        now, now_valid = at_reach(step)
+        before, before_valid = at_reach(step - 1)
+        older, older_valid = at_reach(step - 2)
+        pl.when((step < 2 * reach) & now_valid)(lambda: forward(now))
+        pl.when(step == 0)(lambda: relay(plane))
+        pl.when((step > 0) & (step <= 2 * reach) & before_valid)(lambda: relay(before))
+        settled = jnp.where(step == 1, plane, older)
+        pl.when((step == 1) | ((step > 1) & older_valid))(lambda: own_update(settled))
+        return carry
+
+    lax.fori_loop(0, 2 * reach + 2, gather, 0)
+
+    def result_of(i):
+        return (acc[i, :, :head_size] / acc[i, :, head_size:]).astype(jnp.bfloat16)
+
+    def serve(step, carry):
+        i, valid = at_reach(2 * reach - 1 - step)
+
+        @pl.when(valid)
+        def _():
+            arrival(queries.at[i], z_recv.at[2, i])
+
+            def earlier(p, carry):
                 update(i, p, False)
-
-            @pl.when(i == p)
-            def _():
-                update(i, p, True)
-
-            @pl.when(d == planes - 1)
-            def _():
-                result = (acc[i, :, :head_size] / acc[i, :, head_size:]).astype(jnp.bfloat16)
-
-                @pl.when(t < planes)
-                def _():
-                    results[i] = result
-                    finished(t).start()
-
-                @pl.when(t == planes)
-                def _():
-                    out_ref[:, columns(plane)] = result
-
-            return carry
-
-        lax.fori_loop(1, planes + 1, one, 0)
+                return carry
+
+            lax.fori_loop(0, i, earlier, 0)
+            update(i, i, True)
+            results[i] = result_of(i)
+            finished(i).start()
+
         return carry
 
-    lax.fori_loop(0, planes, step, 0)
-    for t in range(1, planes):
-        query_copy(t).wait_send()
-        for c in pair_copies(t):
+    lax.fori_loop(0, 2 * reach, serve, 0)
+    attended[:, columns(plane)] = result_of(plane)
+    arrival(rim, rim_recv)
+    loads[4].wait()
+
+    for g in range(groups):
+        at = slice(g * head_size, (g + 1) * head_size)
+        window = 2 << (g % 4)
+        before = jnp.where(me > 0, rim[:, at].astype(jnp.float32), 0.0)
+        current = pool_input[:, at].astype(jnp.float32)
+        extended[:WINDOW_MAX, :] = before
+        extended[WINDOW_MAX:, :] = current
+        depth = 1
+        while depth < window:
+            total = extended[depth:, :] + extended[: WINDOW_MAX + rows - depth, :]
+            extended[depth:, :] = total
+            depth = 2 * depth
+        location = me * rows + lax.broadcasted_iota(jnp.int32, (rows, head_size), 0)
+        count = jnp.minimum(window, location + 1).astype(jnp.float32)
+        departure = (extended[WINDOW_MAX:, :] / count - current).astype(jnp.bfloat16)
+        mapped = jnp.dot(departure, pool_weight_ref[g], preferred_element_type=jnp.float32)
+        pooled[:, at] = (mapped * pool_scale_ref[:, at]).astype(jnp.bfloat16)
+
+    chunks = half // (2 * LANES)
+
+    def out_columns(side, c):
+        return pl.ds(pl.multiple_of(side * half + c * 2 * LANES, 2 * LANES), 2 * LANES)
+
+    def chunk_columns(c):
+        return pl.ds(pl.multiple_of(c * 2 * LANES, 2 * LANES), 2 * LANES)
+
+    def pool_part(c, carry):
+        at = chunk_columns(c)
+        whole[:, at] = jnp.dot(pooled[...], outs[0, :, at], preferred_element_type=jnp.float32)
+        return carry
+
+    lax.fori_loop(0, 2 * chunks, pool_part, 0)
+    loads[5].wait()
+    each(range(2 * reach), lambda p: arrival(attended.at[:, columns(p)], o_recv.at[p]))
+
+    def give(c, carry):
+        at = out_columns(1 - core, c)
+        r = whole[:, at] + jnp.dot(attended[...], outs[1, :, at], preferred_element_type=jnp.float32)
+        sent[:, chunk_columns(c)] = r.astype(jnp.bfloat16)
+        return carry
+
+    lax.fori_loop(0, chunks, give, 0)
+    exchange = copy(sent, got, e_send.at[0], e_recv.at[0], sibling)
+    exchange.start()
+
+    def retain(c, carry):
+        at = out_columns(core, c)
+        whole[:, at] = whole[:, at] + jnp.dot(attended[...], outs[1, :, at], preferred_element_type=jnp.float32)
+        return carry
+
+    lax.fori_loop(0, chunks, retain, 0)
+    arrival(got, e_recv.at[0])
+
+    def own_half(at_rows):
+        return whole[at_rows, pl.ds(pl.multiple_of(core * half, half), half)] + got[at_rows, :].astype(jnp.float32)
+
+    def square_rows(n, carry):
+        at = pl.ds(pl.multiple_of(n * SUB_ROWS, SUB_ROWS), SUB_ROWS)
+        mixed = own_half(at)
+        square = mixed * mixed
+        row_sums[core, at, :] = functools.reduce(
+            jnp.add, [square[:, c : c + LANES] for c in range(0, half, LANES)]
+        )
+        return carry
+
+    lax.fori_loop(0, rows // SUB_ROWS, square_rows, 0)
+    sums = copy(row_sums.at[core], row_sums.at[core], e_send.at[1], e_recv.at[1], sibling)
+    sums.start()
+    arrival(row_sums.at[1 - core], e_recv.at[1])
+
+    def finish_rows(n, carry):
+        at = pl.ds(pl.multiple_of(n * SUB_ROWS, SUB_ROWS), SUB_ROWS)
+        total = jnp.sum(row_sums[0, at, :] + row_sums[1, at, :], axis=1, keepdims=True)
+        out_inverse = lax.rsqrt(total / width + epsilon)
+        out_ref[at, :] = (own_half(at) * out_inverse * final_gain_ref[...]).astype(jnp.bfloat16)
+        return carry
+
+    lax.fori_loop(0, rows // SUB_ROWS, finish_rows, 0)
+
+    def drain(p):
+        query_copy(p).wait_send()
+        for n in range(2):
+            tensor_copy(n, p).wait_send()
+            for c in spread(n, p, False):
+                c.wait_send()
+        for c in relays(p):
             c.wait_send()
-    for c in spread(0, True):
+        finished(p).wait_send()
+
+    for n in range(2):
+        for c in spread(n, plane, True):
+            c.wait_send()
+    for c in relays(plane):
         c.wait_send()
-    for t in range(1, planes):
-        for c in spread(t, False):
-            c.wait_send()
-    for t in range(planes):
-        for c in relays(t):
-            c.wait_send()
-    for t in range(1, planes):
-        finished(t).wait_send()
-        arrival(out_ref.at[:, columns(from_plane(t))], o_recv.at[t])
-
-
-def exchange_attend(query, keys, values, log_gates):
-    rows, width = query.shape
+    each(range(2 * reach), drain)
+    for c in swaps + (rim_copy, exchange, sums):
+        c.wait_send()
+
+
+def layer(
+    tokens, input_gain, query_weight, key_weight, value_weight, pool_in_weight, log_gates,
+    pool_weight, pool_scale, attention_out, pooling_out, final_gain,
+):
+    rows, half = tokens.shape
+    width, inner = query_weight.shape
     planes = log_gates.shape[0]
-    seats = lax.axis_size("sp") // planes
-    head_size = width // planes
-    blocks = planes * seats
+    head_size = pool_weight.shape[1]
+    blocks = lax.axis_size("sp")
     dma = pltpu.SemaphoreType.DMA
+    tile = lambda *shape: pltpu.VMEM(shape, jnp.bfloat16)
+    wide = lambda *shape: pltpu.VMEM(shape, jnp.float32)
+    near = pl.BlockSpec(memory_space=pltpu.VMEM)
+    away = pl.BlockSpec(memory_space=pl.ANY)
     pairs = blocks * (blocks + 1) // 2
     return pl.pallas_call(
-        functools.partial(exchange_kernel, planes, seats),
-        out_shape=jax.ShapeDtypeStruct((rows, width), jnp.bfloat16),
-        in_specs=[pl.BlockSpec(memory_space=pltpu.VMEM)] * 4,
-        out_specs=pl.BlockSpec(memory_space=pltpu.VMEM),
+        layer_kernel,
+        out_shape=jax.ShapeDtypeStruct((rows, half), jnp.bfloat16),
+        in_specs=[near, near, away, away, away, away, near, near, near, away, away, near],
+        out_specs=near,
         scratch_shapes=[
-            pltpu.VMEM((blocks * rows, head_size), jnp.bfloat16),
-            pltpu.VMEM((blocks * rows, 2 * head_size), jnp.bfloat16),
-            pltpu.VMEM((planes, rows, head_size), jnp.bfloat16),
-            pltpu.VMEM((planes, rows, head_size), jnp.bfloat16),
-            pltpu.VMEM((planes, rows, 2 * head_size), jnp.float32),
-            pltpu.VMEM((planes, rows, LANES), jnp.float32),
+            tile(4, width, inner), tile(2, inner, width), tile(2, rows, half), wide(2, rows, LANES),
+            wide(rows, LANES), tile(3, rows, inner), tile(WINDOW_MAX, inner), tile(rows, inner),
+            wide(WINDOW_MAX + rows, head_size), tile(rows, inner), wide(rows, width),
+            tile(rows, half), tile(rows, half), wide(2, rows, LANES),
+            tile(blocks * rows, head_size), tile(blocks * rows, 2 * head_size),
+            tile(planes, rows, head_size), tile(planes, rows, head_size), tile(rows, inner),
+            wide(planes, rows, 2 * head_size), wide(planes, rows, LANES),
+            dma((6,)), dma((2,)), dma((2,)), dma((2,)), dma((2,)), dma, dma,
             dma((3, planes)), dma((3, planes)),
             dma((2, planes)), dma((2, planes)),
             dma((2, planes)), dma((2, planes)),
@@ -394,14 +573,17 @@
             dma((planes,)), dma((planes,)),
         ],
         compiler_params=pltpu.CompilerParams(
-            collective_id=0, has_side_effects=True, vmem_limit_bytes=48 * 2**20
+            collective_id=0, has_side_effects=True, vmem_limit_bytes=56 * 2**20
         ),
         cost_estimate=pl.CostEstimate(
-            flops=4 * pairs * rows * rows * head_size,
-            bytes_accessed=2 * 4 * rows * width,
+            flops=4 * pairs * rows * rows * head_size + 12 * rows * width * inner,
+            bytes_accessed=12 * width * inner,
             transcendentals=pairs * rows * rows,
         ),
-    )(query, keys, values, log_gates)
+    )(
+        tokens, input_gain.reshape(1, -1), query_weight, key_weight, value_weight, pool_in_weight, log_gates,
+        pool_weight, pool_scale.reshape(1, -1), attention_out, pooling_out, final_gain.reshape(1, -1),
+    )
 
 
 def ring_attend(query, keys, values, log_gates):
@@ -480,11 +662,17 @@
     groups = pool_weight.shape[0]
     head_size = pool_weight.shape[1]
     heads = log_gates.shape[0]
+    attention_width = query_weight.shape[1]
     pool_width = pool_in_weight.shape[1]
     devices = lax.axis_size("sp")
     shards = lax.axis_size("tp")
     sequence_index = lax.axis_index("sp")
     first_row = sequence_index * tok_rows
+    if shards == 2 and groups % 4 == 0 and heads > 1 and devices == 4 * heads and attention_width == pool_width:
+        return layer(
+            tokens, input_gain, query_weight, key_weight, value_weight, pool_in_weight, log_gates,
+            pool_weight, pool_scale, attention_out, pooling_out, final_gain,
+        )
 
     part = gathered(tokens, "tp")
     gain_part = gathered(input_gain.reshape(1, -1), "tp")
@@ -501,11 +689,7 @@
     pool_input = (product(pool_in_weight) * inverse).astype(jnp.bfloat16)
     rim = passed_along(pool_input[tok_rows - (WINDOW_MAX - 1) :], "sp", 1)
 
-    spread = heads > 1 and devices == 4 * heads
-    if spread:
-        attended = exchange_attend(query, keys, values, log_gates)
-    else:
-        attended = ring_attend(query, keys, values, log_gates)
+    attended = ring_attend(query, keys, values, log_gates)
 
     extended = jnp.concatenate([rim, pool_input], axis=0).astype(jnp.float32)
     column = jnp.arange(pool_width, dtype=jnp.int32)

time: 98.9 us -> 90.2 us (0.912)
  Pallas kernels: 70.8 us -> 86.4 us
  matrix products: 8.2 us -> 0 us
  other arithmetic: 5.82 us -> 0 us
  starting transfers between devices: 5.66 us -> 0 us
  waiting for transfers between devices: 5.28 us -> 0 us
    pallas_call x1, Pallas kernels: 70.8 us -> 86.4 us  [layer(): pl.pallas_call(layer_kernel, out_shape=jax.ShapeDtypeStruct((rows, half),...]
    dot_general x10 -> x0, matrix products: 8.2 us -> none  [the longest x4 5.02 us: product(): return jnp.dot(scaled, weight, preferred_element_type=jnp.float32)]
    ppermute x5 -> x0, starting transfers between devices: 5.66 us -> none  [the longest x1 4.87 us: passed_along(): return lax.ppermute(block, axis, route)]
    ppermute x5 -> x0, waiting for transfers between devices: 5.28 us -> none  [the longest x4 5.28 us: swapped(): lax.ppermute(block, axis, [(i, i ^ offset) for i in range(lax.axis_size(a...]
    convert_element_type x5 -> x0, other arithmetic: 2.34 us -> none  [the longest x1 1.38 us: body(): (mixed * out_inverse[:, None] * final_gain[None, :]).astype(jnp.bfloat16)]
    select_n x2 -> x0, other arithmetic: 2.08 us -> none  [gathered(): jnp.where(lower, block, other)]
    unnamed x20 -> x1, local copies, waits for them, and re-layouts: 1.77 us -> 2.26 us
  transfers between devices with their start and end apart: 5 -> 0, of which waited for: 3 -> 0; matrix products, arithmetic and copies ran while one was open for 7% -> 0% of each run, Pallas kernels for 72% -> 0%
where the time goes in v1:
time: 90.2 us; the launch traced here: 90 us
  Pallas kernels  86.4 us (96%)
  local copies, waits for them, and re-layouts  3.54 us (4%)
    pallas_call x1, Pallas kernels, layer(): pl.pallas_call(layer_kernel, out_shape=jax.ShapeDtypeStruct((rows, half),...  86.4 us
    unnamed x1, local copies, waits for them, and re-layouts  2.26 us

profile of v1, /device:TPU:0, one launch (start us, length us, event | category | flops | bytes accessed | tf_op | source)
XLA Modules:
  0.0 90.0 jit_solution(13855688903681764788)
XLA Ops:
  0.0 1.3 %reshape.9.gain_ref = bf16[1,1024]{1,0:T(2,128)(2,1)} reshape(bf16[1024]{0:T(1024)(128)(2,1)} %param.13) | data formatting | bytes 4096 | tf_op jit(solution)/shard_map/reshape | solution.py:584
  1.3 86.4 %shard_map.118 = bf16[512,1024]{1,0:T(8,128)(2,1)} custom-call(bf16[512,1024]{1,0:T(8,128)(2,1)} %tokens_ref.1, bf16[1,1024]{1,0:T(2,128)(2,1)} %reshape.9.gain_ref, bf16[2048,512]{1,0:T(8,128)(2,1)} %query_weight.1, bf16[2048,512]{1,0:T(8,128)(2,1)} %key_weight.1, bf16[2048,512]{1,0:T(8,128)(2,1)} %value_weight.1, bf16[2048,512]{1,0:T(8,128)(2,1)} %pool_in_weight.1, ...), custom_call_target="tpu_custom_call" | custom-call | flops 24696061952 | bytes 12582912 | tf_op jit(solution)/shard_map/pallas_call | solution.py:555
  87.7 2.3 %copy.14 = bf16[512,1024]{1,0:T(8,128)(2,1)} copy(bf16[512,1024]{1,0:T(8,128)(2,1)} %shard_map.118) | data formatting | bytes 2097152

commit v2 on v1

--- a/solution.py
+++ b/solution.py
@@ -154,10 +154,10 @@
 def layer_kernel(
     tokens_ref, gain_ref, query_weight, key_weight, value_weight, pool_in_weight, gate_ref,
     pool_weight_ref, pool_scale_ref, attention_out, pooling_out, final_gain_ref, out_ref,
-    weights, outs, halves, norms, inverse, made, rim, pool_input, extended, pooled, whole, sent, got, row_sums,
-    keys, values, queries, results, attended, acc, high,
+    weights, outs, halves, norms, inverse, made, parts, rim, pool_input, extended, pooled, whole, sent, got, row_sums,
+    pairs, other_gates, gate_row, queries, results, attended, acc, high,
     w_sem, c_send, c_recv, e_send, e_recv, rim_send, rim_recv,
-    z_send, z_recv, x_send, x_recv, y_send, y_recv, r_send, r_recv, o_send, o_recv,
+    q_send, q_recv, t_send, t_recv, y_send, y_recv, s_send, s_recv, f_send, f_recv, o_send, o_recv,
 ):
     planes, rows, head_size = queries.shape
     width = 2 * halves.shape[2]
@@ -168,10 +168,10 @@
     devices = lax.axis_size("sp")
     seats = devices // planes
     plane, seat = me // seats, me % seats
-    across = seat + 1 - 2 * (seat % 2)
-    along = seat + 2 - 4 * (seat // 2)
-    far = 3 - seat
+    line, side = seat // 2, seat % 2
+    maker = plane % 2
     reach = planes - 1
+    span = seats * rows
 
     loads = [
         pltpu.make_async_copy(source, target, w_sem.at[n])
@@ -185,22 +185,27 @@
     for load in loads:
         load.start()
 
-    def device(p, s):
-        return {"sp": p * seats + s}
+    def device(p, y, x, c):
+        return {"sp": p * seats + 2 * y + x, "tp": c}
 
     sibling = {"tp": 1 - core}
 
-    def block_rows(p, s):
-        return pl.ds(pl.multiple_of((p * seats + s) * rows, rows), rows)
-
-    def columns(p):
-        return pl.ds(pl.multiple_of(p * head_size, head_size), head_size)
-
-    def key_at(p, s):
-        return keys.at[block_rows(p, s), :]
-
-    def value_at(p, s):
-        return values.at[block_rows(p, s), pl.ds(0, head_size)]
+    def columns(l):
+        return pl.ds(pl.multiple_of(l * head_size, head_size), head_size)
+
+    def kept(p, x):
+        return 2 * (p // 2) + x
+
+    own = kept(plane, side)
+
+    def away(p, x, c):
+        return (p != plane) | (x != side) | (c != core)
+
+    def block_rows(p, y, x):
+        return pl.ds(pl.multiple_of((p * seats + 2 * y + x) * rows, rows), rows)
+
+    def block(t, p, y, x):
+        return pairs.at[t, block_rows(p, y, x), pl.ds(0, head_size)]
 
     def copy(source, target, send, recv, to):
         return pltpu.make_async_remote_copy(
@@ -208,18 +213,18 @@
         )
 
     def arrival(target, recv):
-        copy(target, target, z_send.at[0, 0], recv, sibling).wait_recv()
+        copy(target, target, q_send.at[0], recv, sibling).wait_recv()
 
     barrier = pltpu.get_barrier_semaphore()
 
     def greet(to):
         pl.semaphore_signal(barrier, inc=1, device_id=to, device_id_type=MESH)
 
-    for d in range(1, planes):
-        greet(device((plane + d) % planes, seat))
-    greet(device(plane, across))
-    greet(device(plane, along))
-    greet(sibling)
+    for p in range(planes):
+        for x in range(2):
+            for c in range(2):
+                pl.when(away(p, x, c))(functools.partial(greet, device(p, line, x, c)))
+    greet(device(plane, 1 - line, side, core))
     greet({"sp": (me + 1) % devices})
     greet({"sp": (me + devices - 1) % devices})
 
@@ -234,142 +239,172 @@
         return carry
 
     lax.fori_loop(0, rows // SUB_ROWS, scale_rows, 0)
-    pl.semaphore_wait(barrier, planes + 4)
+    pl.semaphore_wait(barrier, 4 * planes + 2)
 
     swaps = (
         copy(halves.at[core], halves.at[core], c_send.at[0], c_recv.at[0], sibling),
         copy(norms.at[core], norms.at[core], c_send.at[1], c_recv.at[1], sibling),
+        copy(gate_ref, other_gates, c_send.at[2], c_recv.at[2], sibling),
     )
     for c in swaps:
         c.start()
-    values[:, head_size:] = jnp.ones((values.shape[0], head_size), values.dtype)
+
+    def project(use):
+        def one(c, carry):
+            use(pl.ds(pl.multiple_of(c * 2 * LANES, 2 * LANES), 2 * LANES))
+            return carry
+
+        lax.fori_loop(0, inner // (2 * LANES), one, 0)
+
+    def product(h, n, at):
+        here = pl.ds(pl.multiple_of(h * half, half), half)
+        return jnp.dot(halves[h], weights[n, here, at], preferred_element_type=jnp.float32)
+
+    for n in range(3):
+        loads[n].wait()
+
+        def begin(at):
+            parts[n, :, at] = product(core, n, at)
+
+        project(begin)
+    pairs[1, :, head_size:] = jnp.ones((pairs.shape[1], head_size), pairs.dtype)
     arrival(norms.at[1 - core], c_recv.at[1])
     total = jnp.sum(norms[0] + norms[1], axis=1, keepdims=True)
     inverse[...] = jnp.broadcast_to(lax.rsqrt(total / width + epsilon), inverse.shape)
     arrival(halves.at[1 - core], c_recv.at[0])
 
-    def project(n, factor, store):
-        loads[n].wait()
-
-        def one(c, carry):
-            at = pl.ds(pl.multiple_of(c * 2 * LANES, 2 * LANES), 2 * LANES)
-            r = jnp.dot(halves[0], weights[n, :half, at], preferred_element_type=jnp.float32)
-            r = r + jnp.dot(halves[1], weights[n, half:, at], preferred_element_type=jnp.float32)
-            f = inverse[...] * factor
-            store(at, (r * jnp.concatenate([f, f], axis=1)).astype(jnp.bfloat16))
-            return carry
-
-        lax.fori_loop(0, inner // (2 * LANES), one, 0)
-
-    def keep(n):
-        def store(at, value):
-            made[n, :, at] = value
-
-        return store
-
-    def at_reach(step):
-        other = plane + (1 + step // 2) * (1 - 2 * (step % 2))
-        return other, (other >= 0) & (other < planes)
-
-    def query_copy(to):
+    def scaled_by(factor, r):
+        f = inverse[...] * factor
+        return (r * jnp.concatenate([f, f], axis=1)).astype(jnp.bfloat16)
+
+    def complete(n, factor):
+        def use(at):
+            made[n, :, at] = scaled_by(factor, parts[n, :, at] + product(1 - core, n, at))
+
+        project(use)
+
+    def query_copy(p, x):
+        l = kept(p, x)
         return copy(
-            made.at[2, :, columns(to)], queries.at[plane], z_send.at[2, to], z_recv.at[2, plane], device(to, seat)
-        )
-
-    def tensor_copy(n, to):
-        target = (key_at, value_at)[n](plane, seat)
-        return copy(made.at[n, :, columns(to)], target, z_send.at[n, to], z_recv.at[n, plane], device(to, seat))
-
-    def spread(n, p, own):
-        target = (key_at, value_at)[n](p, seat)
-        source = made.at[n, :, columns(plane)] if own else target
+            made.at[2, :, columns(l)], queries.at[plane], q_send.at[l], q_recv.at[plane], device(p, line, x, side)
+        )
+
+    def tensor_copy(t, p, x):
+        l = kept(p, x)
+        return copy(
+            made.at[t, :, columns(l)], block(t, plane, line, side),
+            t_send.at[t, l], t_recv.at[2 * plane + side], device(p, line, x, t),
+        )
+
+    served = [2 * n + core for n in range(planes // 2)]
+
+    def send_tensor(t, p, wanted):
+        for x in (side, 1 - side):
+            pl.when(wanted & away(p, x, t))(lambda: tensor_copy(t, p, x).start())
+
+    def send_query(p, wanted):
+        for x in (side, 1 - side):
+            pl.when(wanted & away(p, x, side))(lambda: query_copy(p, x).start())
+
+    def onward(p, x, source):
+        n = 2 * p + x
+        target = block(core, p, line, x)
         return (
-            copy(source, target, x_send.at[n, p], x_recv.at[n, p], device(plane, across)),
-            copy(source, target, y_send.at[n, p], y_recv.at[n, p], device(plane, along)),
-        )
-
-    def relays(p):
-        k, v = key_at(p, across), value_at(p, along)
-        return (
-            copy(k, k, r_send.at[0, p], r_recv.at[0, p], device(plane, along)),
-            copy(v, v, r_send.at[1, p], r_recv.at[1, p], device(plane, across)),
-        )
-
-    def each(steps, action):
-        for step in steps:
-            other, valid = at_reach(step)
-            pl.when(valid)(functools.partial(action, other))
+            copy(source, target, y_send.at[n], y_recv.at[n], device(plane, 1 - line, side, core)),
+            copy(source, target, s_send.at[n], s_recv.at[n], sibling),
+        )
 
     def start_all(copies):
         for c in copies:
             c.start()
 
-    def send_pair(to):
-        start_all((tensor_copy(0, to), tensor_copy(1, to)))
-
-    project(0, 1.0, keep(0))
-    each(range(2), lambda to: tensor_copy(0, to).start())
-    start_all(spread(0, plane, True))
-    project(1, 1.0, keep(1))
-    each(range(2), lambda to: tensor_copy(1, to).start())
-    start_all(spread(1, plane, True))
-    each(range(2, 2 * reach), send_pair)
-    project(2, LOG2E * head_size ** (-0.5), keep(2))
-    each(reversed(range(2 * reach)), lambda to: query_copy(to).start())
-
-    keys[block_rows(plane, seat), :] = made[0, :, columns(plane)]
-    values[block_rows(plane, seat), :head_size] = made[1, :, columns(plane)]
-    queries[plane] = made[2, :, columns(plane)]
+    mine = maker == core
+    complete(0, 1.0)
+    for p in served:
+        send_tensor(0, p, p == plane)
+    send_tensor(0, served[0], served[0] > plane)
+    complete(1, 1.0)
+    for p in served:
+        send_tensor(1, p, p == plane)
+    pl.when(mine)(lambda: start_all(onward(plane, side, made.at[core, :, columns(own)])))
+    send_tensor(1, served[0], served[0] > plane)
+    for p in served[1:]:
+        send_tensor(0, p, p > plane)
+        send_tensor(1, p, p > plane)
+    complete(2, LOG2E * head_size ** (-0.5))
+    for p in served:
+        send_query(p, p <= plane)
+    for p in reversed(served):
+        send_tensor(0, p, p < plane)
+        send_tensor(1, p, p < plane)
+    for p in reversed(served):
+        send_query(p, p > plane)
+
+    @pl.when(mine)
+    def _():
+        pairs[core, block_rows(plane, line, side), :head_size] = made[core, :, columns(own)]
+
+    @pl.when(mine & (side == core))
+    def _():
+        queries[plane] = made[2, :, columns(own)]
+
+    arrival(other_gates, c_recv.at[2])
+    gates = jnp.where(mine, gate_ref[...], other_gates[...])
+    chosen = lax.broadcasted_iota(jnp.int32, gates.shape, 0) == own
+    gate_row[...] = jnp.sum(jnp.where(chosen, gates, 0.0), axis=0, keepdims=True)
     acc[...] = jnp.zeros_like(acc)
     high[...] = jnp.full_like(high, very_low)
 
-    def keep_pool(at, value):
-        pool_input[:, at] = value
-
-    project(3, 1.0, keep_pool)
+    loads[3].wait()
+
+    def pool_product(at):
+        pool_input[:, at] = scaled_by(1.0, product(0, 3, at) + product(1, 3, at))
+
+    project(pool_product)
     rim_copy = copy(
         pool_input.at[pl.ds(rows - WINDOW_MAX, WINDOW_MAX), :], rim, rim_send, rim_recv, {"sp": (me + 1) % devices}
     )
     rim_copy.start()
 
     def forward(p):
-        for n in range(2):
-            arrival((key_at, value_at)[n](p, seat), z_recv.at[n, p])
-            start_all(spread(n, p, False))
+        for x in (side, 1 - side):
+            held = block(core, p, line, x)
+
+            @pl.when(jnp.logical_not(mine & (p == plane) & (x == side)))
+            def _():
+                arrival(held, t_recv.at[2 * p + x])
+                start_all(onward(p, x, held))
+
+    def beside(p, x):
+        n = 2 * p + x
+        held = block(core, p, 1 - line, x)
+        return copy(held, held, f_send.at[n], f_recv.at[n], sibling)
 
     def relay(p):
-        to_along, to_across = relays(p)
-        arrival(key_at(p, across), x_recv.at[0, p])
-        to_along.start()
-        arrival(value_at(p, along), y_recv.at[1, p])
-        to_across.start()
+        for x in (side, 1 - side):
+            arrival(block(core, p, 1 - line, x), y_recv.at[2 * p + x])
+            beside(p, x).start()
 
     def settle(p):
-        arrival(value_at(p, across), x_recv.at[1, p])
-        arrival(key_at(p, along), y_recv.at[0, p])
-        arrival(key_at(p, far), r_recv.at[0, p])
-        arrival(value_at(p, far), r_recv.at[1, p])
-
-    span = seats * rows
-
-    def head_gates(here):
-        block = gate_ref[:, here]
-        mine = lax.broadcasted_iota(jnp.int32, block.shape, 0) == plane
-        return jnp.sum(jnp.where(mine, block, 0.0), axis=0, keepdims=True)
+        for x in range(2):
+            arrival(block(1 - core, p, line, x), s_recv.at[2 * p + x])
+            arrival(block(1 - core, p, 1 - line, x), f_recv.at[2 * p + x])
+
+    place = 2 * line + core
 
     def update(i, p, masked):
         here = pl.ds(pl.multiple_of(p * span, span), span)
-        k = keys[here, :]
-        v = values[here, :]
-        gates = head_gates(here)
-        start = head_gates(pl.ds(pl.multiple_of((i * seats + seat) * rows, rows), LANES))[:, :1]
+        k = pairs[0, here, :head_size]
+        v = pairs[1, here, :]
+        gates = gate_row[:, here]
+        start = gate_row[:, pl.ds(pl.multiple_of((i * seats + place) * rows, rows), LANES)][:, :1]
         bias = (start - gates) * LOG2E
         scores = []
         for r in range(0, rows, SUB_ROWS):
             q = queries[i, r : r + SUB_ROWS, :]
             s = lax.dot_general(q, k, (((1,), (1,)), ((), ())), preferred_element_type=jnp.float32) + bias
             if masked:
-                row = seat * rows + r + lax.broadcasted_iota(jnp.int32, s.shape, 0)
+                row = place * rows + r + lax.broadcasted_iota(jnp.int32, s.shape, 0)
                 s = jnp.where(row >= lax.broadcasted_iota(jnp.int32, s.shape, 1), s, very_low)
             scores.append(s)
         for n, r in enumerate(range(0, rows, SUB_ROWS)):
@@ -383,58 +418,66 @@
             acc[i, at, :] = acc[i, at, :] * jnp.concatenate([factor, factor], axis=1) + summed
             high[i, at, :] = new
 
-    def finished(to):
+    def finished(i):
         return copy(
-            results.at[to], attended.at[:, columns(plane)], o_send.at[to], o_recv.at[plane], device(to, seat)
-        )
-
-    def own_update(p):
-        settle(p)
-
-        @pl.when(p < plane)
-        def _():
-            update(plane, p, False)
-
-        @pl.when(p == plane)
-        def _():
-            update(plane, p, True)
-
-    def gather(step, carry):
-        now, now_valid = at_reach(step)
-        before, before_valid = at_reach(step - 1)
-        older, older_valid = at_reach(step - 2)
-        pl.when((step < 2 * reach) & now_valid)(lambda: forward(now))
-        pl.when(step == 0)(lambda: relay(plane))
-        pl.when((step > 0) & (step <= 2 * reach) & before_valid)(lambda: relay(before))
-        settled = jnp.where(step == 1, plane, older)
-        pl.when((step == 1) | ((step > 1) & older_valid))(lambda: own_update(settled))
-        return carry
-
-    lax.fori_loop(0, 2 * reach + 2, gather, 0)
+            results.at[i], attended.at[:, columns(own)], o_send.at[i], o_recv.at[own], device(i, line, core, maker)
+        )
+
+    def query_arrival(i):
+        pl.when(away(i, core, maker))(lambda: arrival(queries.at[i], q_recv.at[i]))
 
     def result_of(i):
         return (acc[i, :, :head_size] / acc[i, :, head_size:]).astype(jnp.bfloat16)
 
-    def serve(step, carry):
-        i, valid = at_reach(2 * reach - 1 - step)
-
-        @pl.when(valid)
+    def give_back(i):
+        @pl.when(away(i, core, maker))
         def _():
-            arrival(queries.at[i], z_recv.at[2, i])
-
-            def earlier(p, carry):
-                update(i, p, False)
-                return carry
-
-            lax.fori_loop(0, i, earlier, 0)
-            update(i, i, True)
             results[i] = result_of(i)
             finished(i).start()
 
+        @pl.when(jnp.logical_not(away(i, core, maker)))
+        def _():
+            attended[:, columns(own)] = result_of(i)
+
+    def source(n):
+        return jnp.where(n <= plane, plane - n, n)
+
+    def step(n, carry):
+        p = source(n)
+        late = (n == 0) & (plane == 0)
+        more = n < reach
+        relay(p)
+        pl.when(more & jnp.logical_not(late))(lambda: forward(source(n + 1)))
+        settle(p)
+
+        def one(i, carry):
+            pl.when(n == 0)(lambda: query_arrival(i))
+            pl.when(i > p)(lambda: update(i, p, False))
+            pl.when(i == p)(lambda: update(i, p, True))
+            pl.when((i == p) & (i > plane))(lambda: give_back(i))
+            return carry
+
+        lax.fori_loop(jnp.where(p > plane, p, plane), planes, one, 0)
+        pl.when(late)(lambda: forward(source(n + 1)))
         return carry
 
-    lax.fori_loop(0, 2 * reach, serve, 0)
-    attended[:, columns(plane)] = result_of(plane)
+    forward(plane)
+    lax.fori_loop(0, planes, step, 0)
+
+    def serve(i, carry):
+        query_arrival(i)
+
+        def earlier(p, carry):
+            update(i, p, False)
+            return carry
+
+        lax.fori_loop(0, i, earlier, 0)
+        update(i, i, True)
+        give_back(i)
+        return carry
+
+    lax.fori_loop(0, plane, serve, 0)
+    give_back(plane)
     arrival(rim, rim_recv)
     loads[4].wait()
 
@@ -471,7 +514,10 @@
 
     lax.fori_loop(0, 2 * chunks, pool_part, 0)
     loads[5].wait()
-    each(range(2 * reach), lambda p: arrival(attended.at[:, columns(p)], o_recv.at[p]))
+    for p in served:
+        for x in range(2):
+            l = kept(p, x)
+            pl.when(away(p, x, side))(lambda: arrival(attended.at[:, columns(l)], o_recv.at[l]))
 
     def give(c, carry):
         at = out_columns(1 - core, c)
@@ -517,22 +563,17 @@
 
     lax.fori_loop(0, rows // SUB_ROWS, finish_rows, 0)
 
-    def drain(p):
-        query_copy(p).wait_send()
-        for n in range(2):
-            tensor_copy(n, p).wait_send()
-            for c in spread(n, p, False):
+    for p in served:
+        for x in range(2):
+            pl.when(away(p, x, side))(lambda: query_copy(p, x).wait_send())
+            for t in range(2):
+                pl.when(away(p, x, t))(lambda: tensor_copy(t, p, x).wait_send())
+    for p in range(planes):
+        for x in range(2):
+            for c in onward(p, x, block(core, p, line, x)):
                 c.wait_send()
-        for c in relays(p):
-            c.wait_send()
-        finished(p).wait_send()
-
-    for n in range(2):
-        for c in spread(n, plane, True):
-            c.wait_send()
-    for c in relays(plane):
-        c.wait_send()
-    each(range(2 * reach), drain)
+            beside(p, x).wait_send()
+        pl.when(away(p, core, maker))(lambda: finished(p).wait_send())
     for c in swaps + (rim_copy, exchange, sums):
         c.wait_send()
 
@@ -559,17 +600,18 @@
         out_specs=near,
         scratch_shapes=[
             tile(4, width, inner), tile(2, inner, width), tile(2, rows, half), wide(2, rows, LANES),
-            wide(rows, LANES), tile(3, rows, inner), tile(WINDOW_MAX, inner), tile(rows, inner),
+            wide(rows, LANES), tile(3, rows, inner), wide(3, rows, inner), tile(WINDOW_MAX, inner), tile(rows, inner),
             wide(WINDOW_MAX + rows, head_size), tile(rows, inner), wide(rows, width),
             tile(rows, half), tile(rows, half), wide(2, rows, LANES),
-            tile(blocks * rows, head_size), tile(blocks * rows, 2 * head_size),
+            tile(2, blocks * rows, 2 * head_size), wide(*log_gates.shape), wide(1, blocks * rows),
             tile(planes, rows, head_size), tile(planes, rows, head_size), tile(rows, inner),
             wide(planes, rows, 2 * head_size), wide(planes, rows, LANES),
-            dma((6,)), dma((2,)), dma((2,)), dma((2,)), dma((2,)), dma, dma,
-            dma((3, planes)), dma((3, planes)),
-            dma((2, planes)), dma((2, planes)),
-            dma((2, planes)), dma((2, planes)),
-            dma((2, planes)), dma((2, planes)),
+            dma((6,)), dma((3,)), dma((3,)), dma((2,)), dma((2,)), dma, dma,
+            dma((planes,)), dma((planes,)),
+            dma((2, planes)), dma((2 * planes,)),
+            dma((2 * planes,)), dma((2 * planes,)),
+            dma((2 * planes,)), dma((2 * planes,)),
+            dma((2 * planes,)), dma((2 * planes,)),
             dma((planes,)), dma((planes,)),
         ],
         compiler_params=pltpu.CompilerParams(
@@ -668,7 +710,7 @@
     shards = lax.axis_size("tp")
     sequence_index = lax.axis_index("sp")
     first_row = sequence_index * tok_rows
-    if shards == 2 and groups % 4 == 0 and heads > 1 and devices == 4 * heads and attention_width == pool_width:
+    if shards == 2 and groups % 4 == 0 and heads % 2 == 0 and devices == 4 * heads and attention_width == pool_width:
         return layer(
             tokens, input_gain, query_weight, key_weight, value_weight, pool_in_weight, log_gates,
             pool_weight, pool_scale, attention_out, pooling_out, final_gain,

time: 90.2 us -> 83 us (0.920); the launches traced: 90 us -> 81.8 us
  Pallas kernels: 86.4 us -> 78.3 us
    pallas_call x1, Pallas kernels: 86.4 us -> 78.3 us  [layer(): pl.pallas_call(layer_kernel, out_shape=jax.ShapeDtypeStruct((rows, half),...]
where the time goes in v2:
time: 83 us; the launch traced here: 81.8 us
  Pallas kernels  78.3 us (94%)
  local copies, waits for them, and re-layouts  3.54 us (4%)
    pallas_call x1, Pallas kernels, layer(): pl.pallas_call(layer_kernel, out_shape=jax.ShapeDtypeStruct((rows, half),...  78.3 us
    unnamed x1, local copies, waits for them, and re-layouts  2.26 us

profile of v2, /device:TPU:0, one launch (start us, length us, event | category | flops | bytes accessed | tf_op | source)
XLA Modules:
  0.0 81.8 jit_solution(17421962476907880451)
XLA Ops:
  0.0 1.3 %reshape.9.gain_ref = bf16[1,1024]{1,0:T(2,128)(2,1)} reshape(bf16[1024]{0:T(1024)(128)(2,1)} %param.13) | data formatting | bytes 4096 | tf_op jit(solution)/shard_map/reshape | solution.py:626
  1.3 78.3 %shard_map.118 = bf16[512,1024]{1,0:T(8,128)(2,1)} custom-call(bf16[512,1024]{1,0:T(8,128)(2,1)} %tokens_ref.1, bf16[1,1024]{1,0:T(2,128)(2,1)} %reshape.9.gain_ref, bf16[2048,512]{1,0:T(8,128)(2,1)} %query_weight.1, bf16[2048,512]{1,0:T(8,128)(2,1)} %key_weight.1, bf16[2048,512]{1,0:T(8,128)(2,1)} %value_weight.1, bf16[2048,512]{1,0:T(8,128)(2,1)} %pool_in_weight.1, ...), custom_call_target="tpu_custom_call" | custom-call | flops 24696061952 | bytes 12582912 | tf_op jit(solution)/shard_map/pallas_call | solution.py:596
  79.5 2.3 %copy.14 = bf16[512,1024]{1,0:T(8,128)(2,1)} copy(bf16[512,1024]{1,0:T(8,128)(2,1)} %shard_map.118) | data formatting | bytes 2097152

commit v3 on v2

--- a/solution.py
+++ b/solution.py
@@ -149,14 +149,15 @@
 
 MESH = pl.DeviceIdType.MESH
 SUB_ROWS = 128
+PIECES = 2
 
 
 def layer_kernel(
     tokens_ref, gain_ref, query_weight, key_weight, value_weight, pool_in_weight, gate_ref,
     pool_weight_ref, pool_scale_ref, attention_out, pooling_out, final_gain_ref, out_ref,
-    weights, outs, halves, norms, inverse, made, parts, rim, pool_input, extended, pooled, whole, sent, got, row_sums,
+    held_tokens, weights, outs, halves, norms, inverse, made, parts, rim, pool_input, extended, pooled, whole, foreign, row_sums,
     pairs, other_gates, gate_row, queries, results, attended, acc, high,
-    w_sem, c_send, c_recv, e_send, e_recv, rim_send, rim_recv,
+    w_sem, c_send, c_recv, e_send, e_recv, p_send, p_recv, rim_send, rim_recv,
     q_send, q_recv, t_send, t_recv, y_send, y_recv, s_send, s_recv, f_send, f_recv, o_send, o_recv,
 ):
     planes, rows, head_size = queries.shape
@@ -173,6 +174,8 @@
     reach = planes - 1
     span = seats * rows
 
+    tokens_load = pltpu.make_async_copy(tokens_ref, held_tokens, w_sem.at[6])
+    tokens_load.start()
     loads = [
         pltpu.make_async_copy(source, target, w_sem.at[n])
         for n, (source, target) in enumerate(
@@ -204,8 +207,11 @@
     def block_rows(p, y, x):
         return pl.ds(pl.multiple_of((p * seats + 2 * y + x) * rows, rows), rows)
 
-    def block(t, p, y, x):
-        return pairs.at[t, block_rows(p, y, x), pl.ds(0, head_size)]
+    piece = rows // PIECES
+
+    def block(t, p, y, x, h):
+        at = pl.multiple_of((p * seats + 2 * y + x) * rows + h * piece, piece)
+        return pairs.at[t, pl.ds(at, piece), pl.ds(0, head_size)]
 
     def copy(source, target, send, recv, to):
         return pltpu.make_async_remote_copy(
@@ -230,14 +236,15 @@
 
     def scale_rows(n, carry):
         at = pl.ds(pl.multiple_of(n * SUB_ROWS, SUB_ROWS), SUB_ROWS)
-        widened = tokens_ref[at, :].astype(jnp.float32)
-        halves[core, at, :] = (widened * gain_ref[...].astype(jnp.float32)).astype(jnp.bfloat16)
+        widened = held_tokens[at, :].astype(jnp.float32)
+        halves[core, at, :] = (widened * gain_ref[...].astype(jnp.float32).reshape(1, half)).astype(jnp.bfloat16)
         square = widened * widened
         norms[core, at, :] = functools.reduce(
             jnp.add, [square[:, c : c + LANES] for c in range(0, half, LANES)]
         )
         return carry
 
+    tokens_load.wait()
     lax.fori_loop(0, rows // SUB_ROWS, scale_rows, 0)
     pl.semaphore_wait(barrier, 4 * planes + 2)
 
@@ -283,40 +290,57 @@
 
         project(use)
 
+    def start_all(copies):
+        for c in copies:
+            c.start()
+
     def query_copy(p, x):
         l = kept(p, x)
         return copy(
             made.at[2, :, columns(l)], queries.at[plane], q_send.at[l], q_recv.at[plane], device(p, line, x, side)
         )
 
-    def tensor_copy(t, p, x):
+    def tensor_copies(t, p, x):
         l = kept(p, x)
-        return copy(
-            made.at[t, :, columns(l)], block(t, plane, line, side),
-            t_send.at[t, l], t_recv.at[2 * plane + side], device(p, line, x, t),
-        )
+        return [
+            copy(
+                made.at[t, pl.ds(h * piece, piece), columns(l)], block(t, plane, line, side, h),
+                t_send.at[t, l, h], t_recv.at[2 * plane + side, h], device(p, line, x, t),
+            )
+            for h in range(PIECES)
+        ]
 
     served = [2 * n + core for n in range(planes // 2)]
+    middle = planes // 2
+    upper = plane >= middle
+
+    def crossing(p):
+        return (p >= middle) != upper
+
+    def wait_all(copies):
+        for c in copies:
+            c.wait_send()
 
     def send_tensor(t, p, wanted):
         for x in (side, 1 - side):
-            pl.when(wanted & away(p, x, t))(lambda: tensor_copy(t, p, x).start())
+            pl.when(wanted & away(p, x, t))(lambda: start_all(tensor_copies(t, p, x)))
 
     def send_query(p, wanted):
         for x in (side, 1 - side):
             pl.when(wanted & away(p, x, side))(lambda: query_copy(p, x).start())
 
-    def onward(p, x, source):
+    def onward(p, x, h, source=None):
         n = 2 * p + x
-        target = block(core, p, line, x)
+        target = block(core, p, line, x, h)
+        source = target if source is None else source
         return (
-            copy(source, target, y_send.at[n], y_recv.at[n], device(plane, 1 - line, side, core)),
-            copy(source, target, s_send.at[n], s_recv.at[n], sibling),
+            copy(source, target, y_send.at[n, h], y_recv.at[n, h], device(plane, 1 - line, side, core)),
+            copy(source, target, s_send.at[n, h], s_recv.at[n, h], sibling),
         )
 
-    def start_all(copies):
-        for c in copies:
-            c.start()
+    def onward_own():
+        for h in range(PIECES):
+            start_all(onward(plane, side, h, made.at[core, pl.ds(h * piece, piece), columns(own)]))
 
     mine = maker == core
     complete(0, 1.0)
@@ -326,19 +350,39 @@
     complete(1, 1.0)
     for p in served:
         send_tensor(1, p, p == plane)
-    pl.when(mine)(lambda: start_all(onward(plane, side, made.at[core, :, columns(own)])))
+    pl.when(mine)(onward_own)
     send_tensor(1, served[0], served[0] > plane)
     for p in served[1:]:
         send_tensor(0, p, p > plane)
         send_tensor(1, p, p > plane)
     complete(2, LOG2E * head_size ** (-0.5))
     for p in served:
-        send_query(p, p <= plane)
-    for p in reversed(served):
-        send_tensor(0, p, p < plane)
-        send_tensor(1, p, p < plane)
-    for p in reversed(served):
-        send_query(p, p > plane)
+        send_query(p, jnp.logical_not(crossing(p)) | upper)
+    for p in served:
+        for t in range(2):
+            send_tensor(t, p, (p < plane) & jnp.logical_not(crossing(p)))
+
+    for p in served:
+        send_query(p, crossing(p) & jnp.logical_not(upper))
+
+    def over_crossing(action):
+        for p in served:
+            for x in (side, 1 - side):
+                pl.when(crossing(p))(functools.partial(action, p, x))
+
+    def release_keys():
+        def action(p, x):
+            query_copy(p, x).wait_send()
+            start_all(tensor_copies(0, p, x))
+
+        over_crossing(action)
+
+    def release_values():
+        def action(p, x):
+            wait_all(tensor_copies(0, p, x))
+            start_all(tensor_copies(1, p, x))
+
+        over_crossing(action)
 
     @pl.when(mine)
     def _():
@@ -368,27 +412,29 @@
 
     def forward(p):
         for x in (side, 1 - side):
-            held = block(core, p, line, x)
 
             @pl.when(jnp.logical_not(mine & (p == plane) & (x == side)))
             def _():
-                arrival(held, t_recv.at[2 * p + x])
-                start_all(onward(p, x, held))
-
-    def beside(p, x):
+                for h in range(PIECES):
+                    arrival(block(core, p, line, x, h), t_recv.at[2 * p + x, h])
+                    start_all(onward(p, x, h))
+
+    def beside(p, x, h):
         n = 2 * p + x
-        held = block(core, p, 1 - line, x)
-        return copy(held, held, f_send.at[n], f_recv.at[n], sibling)
+        held = block(core, p, 1 - line, x, h)
+        return copy(held, held, f_send.at[n, h], f_recv.at[n, h], sibling)
 
     def relay(p):
         for x in (side, 1 - side):
-            arrival(block(core, p, 1 - line, x), y_recv.at[2 * p + x])
-            beside(p, x).start()
+            for h in range(PIECES):
+                arrival(block(core, p, 1 - line, x, h), y_recv.at[2 * p + x, h])
+                beside(p, x, h).start()
 
     def settle(p):
         for x in range(2):
-            arrival(block(1 - core, p, line, x), s_recv.at[2 * p + x])
-            arrival(block(1 - core, p, 1 - line, x), f_recv.at[2 * p + x])
+            for h in range(PIECES):
+                arrival(block(1 - core, p, line, x, h), s_recv.at[2 * p + x, h])
+                arrival(block(1 - core, p, 1 - line, x, h), f_recv.at[2 * p + x, h])
 
     place = 2 * line + core
 
@@ -420,7 +466,7 @@
 
     def finished(i):
         return copy(
-            results.at[i], attended.at[:, columns(own)], o_send.at[i], o_recv.at[own], device(i, line, core, maker)
+            results.at[i], attended.at[maker, :, columns(own)], o_send.at[i], o_recv.at[own], device(i, line, core, maker)
         )
 
     def query_arrival(i):
@@ -437,16 +483,44 @@
 
         @pl.when(jnp.logical_not(away(i, core, maker)))
         def _():
-            attended[:, columns(own)] = result_of(i)
+            attended[core, :, columns(own)] = result_of(i)
 
     def source(n):
-        return jnp.where(n <= plane, plane - n, n)
+        base = plane // middle * middle
+        near = base + (plane - base + n) % middle
+        return jnp.where(n < middle, near, jnp.where(upper, reach - n, n))
+
+    pooled_copy = copy(pooled.at[core], pooled.at[core], e_send.at[0], e_recv.at[0], sibling)
+
+    def pool():
+        arrival(rim, rim_recv)
+
+        for g in range(groups):
+            at = slice(g * head_size, (g + 1) * head_size)
+            window = 2 << (g % 4)
+            before = jnp.where(me > 0, rim[:, at].astype(jnp.float32), 0.0)
+            current = pool_input[:, at].astype(jnp.float32)
+            extended[:WINDOW_MAX, :] = before
+            extended[WINDOW_MAX:, :] = current
+            depth = 1
+            while depth < window:
+                total = extended[depth:, :] + extended[: WINDOW_MAX + rows - depth, :]
+                extended[depth:, :] = total
+                depth = 2 * depth
+            location = me * rows + lax.broadcasted_iota(jnp.int32, (rows, head_size), 0)
+            count = jnp.minimum(window, location + 1).astype(jnp.float32)
+            departure = (extended[WINDOW_MAX:, :] / count - current).astype(jnp.bfloat16)
+            mapped = jnp.dot(departure, pool_weight_ref[g], preferred_element_type=jnp.float32)
+            pooled[core, :, at] = (mapped * pool_scale_ref[:, at]).astype(jnp.bfloat16)
+
+        pooled_copy.start()
 
     def step(n, carry):
         p = source(n)
-        late = (n == 0) & (plane == 0)
+        late = n == middle - 1
         more = n < reach
         relay(p)
+        pl.when(upper & (n == 0))(release_keys)
         pl.when(more & jnp.logical_not(late))(lambda: forward(source(n + 1)))
         settle(p)
 
@@ -454,14 +528,20 @@
             pl.when(n == 0)(lambda: query_arrival(i))
             pl.when(i > p)(lambda: update(i, p, False))
             pl.when(i == p)(lambda: update(i, p, True))
-            pl.when((i == p) & (i > plane))(lambda: give_back(i))
+            pl.when((i > plane) & jnp.where(upper, n == reach, i == p))(lambda: give_back(i))
             return carry
 
         lax.fori_loop(jnp.where(p > plane, p, plane), planes, one, 0)
-        pl.when(late)(lambda: forward(source(n + 1)))
+        pl.when(upper & (n == middle - 1))(release_values)
+        pl.when(more & late)(lambda: forward(source(n + 1)))
         return carry
 
     forward(plane)
+    loads[4].wait()
+    loads[5].wait()
+    theirs = pl.ds(pl.multiple_of((1 - core) * half, half), half)
+    shared = [copy(outs.at[n, :, theirs], foreign.at[n], e_send.at[2 + n], e_recv.at[2 + n], sibling) for n in range(2)]
+    start_all(shared)
     lax.fori_loop(0, planes, step, 0)
 
     def serve(i, carry):
@@ -478,71 +558,65 @@
 
     lax.fori_loop(0, plane, serve, 0)
     give_back(plane)
-    arrival(rim, rim_recv)
-    loads[4].wait()
-
-    for g in range(groups):
-        at = slice(g * head_size, (g + 1) * head_size)
-        window = 2 << (g % 4)
-        before = jnp.where(me > 0, rim[:, at].astype(jnp.float32), 0.0)
-        current = pool_input[:, at].astype(jnp.float32)
-        extended[:WINDOW_MAX, :] = before
-        extended[WINDOW_MAX:, :] = current
-        depth = 1
-        while depth < window:
-            total = extended[depth:, :] + extended[: WINDOW_MAX + rows - depth, :]
-            extended[depth:, :] = total
-            depth = 2 * depth
-        location = me * rows + lax.broadcasted_iota(jnp.int32, (rows, head_size), 0)
-        count = jnp.minimum(window, location + 1).astype(jnp.float32)
-        departure = (extended[WINDOW_MAX:, :] / count - current).astype(jnp.bfloat16)
-        mapped = jnp.dot(departure, pool_weight_ref[g], preferred_element_type=jnp.float32)
-        pooled[:, at] = (mapped * pool_scale_ref[:, at]).astype(jnp.bfloat16)
+    pool()
 
     chunks = half // (2 * LANES)
-
-    def out_columns(side, c):
-        return pl.ds(pl.multiple_of(side * half + c * 2 * LANES, 2 * LANES), 2 * LANES)
 
     def chunk_columns(c):
         return pl.ds(pl.multiple_of(c * 2 * LANES, 2 * LANES), 2 * LANES)
 
+    def home_columns(c):
+        return pl.ds(pl.multiple_of(core * half + c * 2 * LANES, 2 * LANES), 2 * LANES)
+
+    for n in range(2):
+        arrival(foreign.at[n], e_recv.at[2 + n])
+
     def pool_part(c, carry):
         at = chunk_columns(c)
-        whole[:, at] = jnp.dot(pooled[...], outs[0, :, at], preferred_element_type=jnp.float32)
+        whole[:, at] = jnp.dot(pooled[core], outs[0, :, home_columns(c)], preferred_element_type=jnp.float32)
         return carry
 
-    lax.fori_loop(0, 2 * chunks, pool_part, 0)
-    loads[5].wait()
+    def pool_rest(c, carry):
+        at = chunk_columns(c)
+        r = jnp.dot(pooled[1 - core], foreign[0, :, at], preferred_element_type=jnp.float32)
+        whole[:, at] = whole[:, at] + r
+        return carry
+
+    lax.fori_loop(0, chunks, pool_part, 0)
+    arrival(pooled.at[1 - core], e_recv.at[0])
+    lax.fori_loop(0, chunks, pool_rest, 0)
+
+    def pass_on(l):
+        held = attended.at[core, :, columns(l)]
+        return copy(held, held, p_send.at[l], p_recv.at[l], sibling)
+
     for p in served:
         for x in range(2):
             l = kept(p, x)
-            pl.when(away(p, x, side))(lambda: arrival(attended.at[:, columns(l)], o_recv.at[l]))
-
-    def give(c, carry):
-        at = out_columns(1 - core, c)
-        r = whole[:, at] + jnp.dot(attended[...], outs[1, :, at], preferred_element_type=jnp.float32)
-        sent[:, chunk_columns(c)] = r.astype(jnp.bfloat16)
+            pl.when(away(p, x, side))(lambda: arrival(attended.at[core, :, columns(l)], o_recv.at[l]))
+            pass_on(l).start()
+
+    def retain(c, carry):
+        at = chunk_columns(c)
+        r = jnp.dot(attended[core], outs[1, :, home_columns(c)], preferred_element_type=jnp.float32)
+        whole[:, at] = whole[:, at] + r
         return carry
 
-    lax.fori_loop(0, chunks, give, 0)
-    exchange = copy(sent, got, e_send.at[0], e_recv.at[0], sibling)
-    exchange.start()
-
-    def retain(c, carry):
-        at = out_columns(core, c)
-        whole[:, at] = whole[:, at] + jnp.dot(attended[...], outs[1, :, at], preferred_element_type=jnp.float32)
+    lax.fori_loop(0, chunks, retain, 0)
+    for l in range(planes):
+        arrival(attended.at[1 - core, :, columns(l)], p_recv.at[l])
+
+    def add(c, carry):
+        at = chunk_columns(c)
+        r = jnp.dot(attended[1 - core], foreign[1, :, at], preferred_element_type=jnp.float32)
+        whole[:, at] = whole[:, at] + r
         return carry
 
-    lax.fori_loop(0, chunks, retain, 0)
-    arrival(got, e_recv.at[0])
-
-    def own_half(at_rows):
-        return whole[at_rows, pl.ds(pl.multiple_of(core * half, half), half)] + got[at_rows, :].astype(jnp.float32)
+    lax.fori_loop(0, chunks, add, 0)
 
     def square_rows(n, carry):
         at = pl.ds(pl.multiple_of(n * SUB_ROWS, SUB_ROWS), SUB_ROWS)
-        mixed = own_half(at)
+        mixed = whole[at, :]
         square = mixed * mixed
         row_sums[core, at, :] = functools.reduce(
             jnp.add, [square[:, c : c + LANES] for c in range(0, half, LANES)]
@@ -558,23 +632,29 @@
         at = pl.ds(pl.multiple_of(n * SUB_ROWS, SUB_ROWS), SUB_ROWS)
         total = jnp.sum(row_sums[0, at, :] + row_sums[1, at, :], axis=1, keepdims=True)
         out_inverse = lax.rsqrt(total / width + epsilon)
-        out_ref[at, :] = (own_half(at) * out_inverse * final_gain_ref[...]).astype(jnp.bfloat16)
+        out_ref[at, :] = (whole[at, :] * out_inverse * final_gain_ref[...]).astype(jnp.bfloat16)
         return carry
 
     lax.fori_loop(0, rows // SUB_ROWS, finish_rows, 0)
 
     for p in served:
         for x in range(2):
-            pl.when(away(p, x, side))(lambda: query_copy(p, x).wait_send())
-            for t in range(2):
-                pl.when(away(p, x, t))(lambda: tensor_copy(t, p, x).wait_send())
+            waited = crossing(p)
+            left = (
+                (lambda: query_copy(p, x).wait_send(), waited & upper, side),
+                (lambda: wait_all(tensor_copies(0, p, x)), waited & upper, 0),
+                (lambda: wait_all(tensor_copies(1, p, x)), False, 1),
+            )
+            for action, done, c in left:
+                pl.when(away(p, x, c) & jnp.logical_not(done))(action)
     for p in range(planes):
         for x in range(2):
-            for c in onward(p, x, block(core, p, line, x)):
-                c.wait_send()
-            beside(p, x).wait_send()
+            for h in range(PIECES):
+                for c in onward(p, x, h):
+                    c.wait_send()
+                beside(p, x, h).wait_send()
         pl.when(away(p, core, maker))(lambda: finished(p).wait_send())
-    for c in swaps + (rim_copy, exchange, sums):
+    for c in [*swaps, *shared, rim_copy, pooled_copy, sums] + [pass_on(l) for l in range(planes)]:
         c.wait_send()
 
 
@@ -596,22 +676,22 @@
     return pl.pallas_call(
         layer_kernel,
         out_shape=jax.ShapeDtypeStruct((rows, half), jnp.bfloat16),
-        in_specs=[near, near, away, away, away, away, near, near, near, away, away, near],
+        in_specs=[away, near, away, away, away, away, near, near, near, away, away, near],
         out_specs=near,
         scratch_shapes=[
-            tile(4, width, inner), tile(2, inner, width), tile(2, rows, half), wide(2, rows, LANES),
+            tile(rows, half), tile(4, width, inner), tile(2, inner, width), tile(2, rows, half), wide(2, rows, LANES),
             wide(rows, LANES), tile(3, rows, inner), wide(3, rows, inner), tile(WINDOW_MAX, inner), tile(rows, inner),
-            wide(WINDOW_MAX + rows, head_size), tile(rows, inner), wide(rows, width),
-            tile(rows, half), tile(rows, half), wide(2, rows, LANES),
+            wide(WINDOW_MAX + rows, head_size), tile(2, rows, inner), wide(rows, half),
+            tile(2, inner, half), wide(2, rows, LANES),
             tile(2, blocks * rows, 2 * head_size), wide(*log_gates.shape), wide(1, blocks * rows),
-            tile(planes, rows, head_size), tile(planes, rows, head_size), tile(rows, inner),
+            tile(planes, rows, head_size), tile(planes, rows, head_size), tile(2, rows, inner),
             wide(planes, rows, 2 * head_size), wide(planes, rows, LANES),
-            dma((6,)), dma((3,)), dma((3,)), dma((2,)), dma((2,)), dma, dma,
+            dma((7,)), dma((3,)), dma((3,)), dma((4,)), dma((4,)), dma((planes,)), dma((planes,)), dma, dma,
             dma((planes,)), dma((planes,)),
-            dma((2, planes)), dma((2 * planes,)),
-            dma((2 * planes,)), dma((2 * planes,)),
-            dma((2 * planes,)), dma((2 * planes,)),
-            dma((2 * planes,)), dma((2 * planes,)),
+            dma((2, planes, PIECES)), dma((2 * planes, PIECES)),
+            dma((2 * planes, PIECES)), dma((2 * planes, PIECES)),
+            dma((2 * planes, PIECES)), dma((2 * planes, PIECES)),
+            dma((2 * planes, PIECES)), dma((2 * planes, PIECES)),
             dma((planes,)), dma((planes,)),
         ],
         compiler_params=pltpu.CompilerParams(
@@ -623,7 +703,7 @@
             transcendentals=pairs * rows * rows,
         ),
     )(
-        tokens, input_gain.reshape(1, -1), query_weight, key_weight, value_weight, pool_in_weight, log_gates,
+        tokens, input_gain, query_weight, key_weight, value_weight, pool_in_weight, log_gates,
         pool_weight, pool_scale.reshape(1, -1), attention_out, pooling_out, final_gain.reshape(1, -1),
     )
 

time: 83 us -> 77.7 us (0.936); the launches traced: 81.8 us -> 77.6 us
  Pallas kernels: 78.3 us -> 75.3 us
  local copies, waits for them, and re-layouts: 3.54 us -> 2.26 us
    pallas_call x1, Pallas kernels: 78.3 us -> 75.3 us  [layer(): pl.pallas_call(layer_kernel, out_shape=jax.ShapeDtypeStruct((rows, half),...]
    reshape x1 -> x0, local copies, waits for them, and re-layouts: 1.28 us -> none  [layer(): input_gain.reshape(1, -1)]
where the time goes in v3:
time: 77.7 us; the launch traced here: 77.6 us
  Pallas kernels  75.3 us (97%)
  local copies, waits for them, and re-layouts  2.26 us (3%)
    pallas_call x1, Pallas kernels, layer(): pl.pallas_call(layer_kernel, out_shape=jax.ShapeDtypeStruct((rows, half),...  75.3 us
    unnamed x1, local copies, waits for them, and re-layouts  2.26 us

profile of v3, /device:TPU:0, one launch (start us, length us, event | category | flops | bytes accessed | tf_op | source)
XLA Modules:
  0.0 77.6 jit_solution(205265510048607763)
XLA Ops:
  0.0 75.3 %shard_map.118 = bf16[512,1024]{1,0:T(8,128)(2,1)} custom-call(bf16[512,1024]{1,0:T(8,128)(2,1)} %tokens_ref.1, bf16[1024]{0:T(1024)(128)(2,1)} %gain_ref.1, bf16[2048,512]{1,0:T(8,128)(2,1)} %query_weight.1, bf16[2048,512]{1,0:T(8,128)(2,1)} %key_weight.1, bf16[2048,512]{1,0:T(8,128)(2,1)} %value_weight.1, bf16[2048,512]{1,0:T(8,128)(2,1)} %pool_in_weight.1, ...), custom_call_target="tpu_custom_call" | custom-call | flops 24696061952 | bytes 12582912 | tf_op jit(solution)/shard_map/pallas_call | solution.py:676
  75.3 2.3 %copy.14 = bf16[512,1024]{1,0:T(8,128)(2,1)} copy(bf16[512,1024]{1,0:T(8,128)(2,1)} %shard_map.118) | data formatting | bytes 2097152

commit v4 on v3

--- a/solution.py
+++ b/solution.py
@@ -155,9 +155,9 @@
 def layer_kernel(
     tokens_ref, gain_ref, query_weight, key_weight, value_weight, pool_in_weight, gate_ref,
     pool_weight_ref, pool_scale_ref, attention_out, pooling_out, final_gain_ref, out_ref,
-    held_tokens, weights, outs, halves, norms, inverse, made, parts, rim, pool_input, extended, pooled, whole, foreign, row_sums,
+    held_tokens, finished_rows, weights, outs, halves, norms, inverse, made, parts, rim, pool_input, extended, pooled, whole, foreign, row_sums,
     pairs, other_gates, gate_row, queries, results, attended, acc, high,
-    w_sem, c_send, c_recv, e_send, e_recv, p_send, p_recv, rim_send, rim_recv,
+    w_sem, f_sem, c_send, c_recv, e_send, e_recv, p_send, p_recv, rim_send, rim_recv,
     q_send, q_recv, t_send, t_recv, y_send, y_recv, s_send, s_recv, f_send, f_recv, o_send, o_recv,
 ):
     planes, rows, head_size = queries.shape
@@ -518,10 +518,9 @@
     def step(n, carry):
         p = source(n)
         late = n == middle - 1
-        more = n < reach
         relay(p)
         pl.when(upper & (n == 0))(release_keys)
-        pl.when(more & jnp.logical_not(late))(lambda: forward(source(n + 1)))
+        pl.when(n < middle - 1)(lambda: forward(source(n + 1)))
         settle(p)
 
         def one(i, carry):
@@ -533,7 +532,12 @@
 
         lax.fori_loop(jnp.where(p > plane, p, plane), planes, one, 0)
         pl.when(upper & (n == middle - 1))(release_values)
-        pl.when(more & late)(lambda: forward(source(n + 1)))
+
+        @pl.when(late)
+        def _():
+            for m in range(middle, planes):
+                forward(source(m))
+
         return carry
 
     forward(plane)
@@ -628,11 +632,16 @@
     sums.start()
     arrival(row_sums.at[1 - core], e_recv.at[1])
 
+    def out_copy(n):
+        at = pl.ds(pl.multiple_of(n * SUB_ROWS, SUB_ROWS), SUB_ROWS)
+        return pltpu.make_async_copy(finished_rows.at[at, :], out_ref.at[at, :], f_sem.at[n])
+
     def finish_rows(n, carry):
         at = pl.ds(pl.multiple_of(n * SUB_ROWS, SUB_ROWS), SUB_ROWS)
         total = jnp.sum(row_sums[0, at, :] + row_sums[1, at, :], axis=1, keepdims=True)
         out_inverse = lax.rsqrt(total / width + epsilon)
-        out_ref[at, :] = (whole[at, :] * out_inverse * final_gain_ref[...]).astype(jnp.bfloat16)
+        finished_rows[at, :] = (whole[at, :] * out_inverse * final_gain_ref[...]).astype(jnp.bfloat16)
+        out_copy(n).start()
         return carry
 
     lax.fori_loop(0, rows // SUB_ROWS, finish_rows, 0)
@@ -656,6 +665,8 @@
         pl.when(away(p, core, maker))(lambda: finished(p).wait_send())
     for c in [*swaps, *shared, rim_copy, pooled_copy, sums] + [pass_on(l) for l in range(planes)]:
         c.wait_send()
+    for n in range(rows // SUB_ROWS):
+        out_copy(n).wait()
 
 
 def layer(
@@ -677,16 +688,16 @@
         layer_kernel,
         out_shape=jax.ShapeDtypeStruct((rows, half), jnp.bfloat16),
         in_specs=[away, near, away, away, away, away, near, near, near, away, away, near],
-        out_specs=near,
+        out_specs=away,
         scratch_shapes=[
-            tile(rows, half), tile(4, width, inner), tile(2, inner, width), tile(2, rows, half), wide(2, rows, LANES),
+            tile(rows, half), tile(rows, half), tile(4, width, inner), tile(2, inner, width), tile(2, rows, half), wide(2, rows, LANES),
             wide(rows, LANES), tile(3, rows, inner), wide(3, rows, inner), tile(WINDOW_MAX, inner), tile(rows, inner),
             wide(WINDOW_MAX + rows, head_size), tile(2, rows, inner), wide(rows, half),
             tile(2, inner, half), wide(2, rows, LANES),
             tile(2, blocks * rows, 2 * head_size), wide(*log_gates.shape), wide(1, blocks * rows),
             tile(planes, rows, head_size), tile(planes, rows, head_size), tile(2, rows, inner),
             wide(planes, rows, 2 * head_size), wide(planes, rows, LANES),
-            dma((7,)), dma((3,)), dma((3,)), dma((4,)), dma((4,)), dma((planes,)), dma((planes,)), dma, dma,
+            dma((7,)), dma((rows // SUB_ROWS,)), dma((3,)), dma((3,)), dma((4,)), dma((4,)), dma((planes,)), dma((planes,)), dma, dma,
             dma((planes,)), dma((planes,)),
             dma((2, planes, PIECES)), dma((2 * planes, PIECES)),
             dma((2 * planes, PIECES)), dma((2 * planes, PIECES)),

time: 77.7 us -> 77 us (level)
  Pallas kernels: 75.3 us -> 74.5 us
where the time goes in v4:
time: 77 us; the launch traced here: 76.8 us
  Pallas kernels  74.5 us (97%)
  local copies, waits for them, and re-layouts  2.26 us (3%)
    pallas_call x1, Pallas kernels, layer(): pl.pallas_call(layer_kernel, out_shape=jax.ShapeDtypeStruct((rows, half),...  74.5 us
    unnamed x1, local copies, waits for them, and re-layouts  2.26 us

profile of v4, /device:TPU:0, one launch (start us, length us, event | category | flops | bytes accessed | tf_op | source)
XLA Modules:
  0.0 76.8 jit_solution(18041646559252823315)
XLA Ops:
  0.0 74.5 %shard_map.118 = bf16[512,1024]{1,0:T(8,128)(2,1)} custom-call(bf16[512,1024]{1,0:T(8,128)(2,1)} %tokens_ref.1, bf16[1024]{0:T(1024)(128)(2,1)} %gain_ref.1, bf16[2048,512]{1,0:T(8,128)(2,1)} %query_weight.1, bf16[2048,512]{1,0:T(8,128)(2,1)} %key_weight.1, bf16[2048,512]{1,0:T(8,128)(2,1)} %value_weight.1, bf16[2048,512]{1,0:T(8,128)(2,1)} %pool_in_weight.1, ...), custom_call_target="tpu_custom_call" | custom-call | flops 24696061952 | bytes 12582912 | tf_op jit(solution)/shard_map/pallas_call | solution.py:687
  74.6 2.3 %copy.14 = bf16[512,1024]{1,0:T(8,128)(2,1)} copy(bf16[512,1024]{1,0:T(8,128)(2,1)} %shard_map.118) | data formatting | bytes 2097152
